TPU v7x, 32 devices: a whole 2x2x4 slice. The times are simulated.
32 devices in a mesh: sp: 16 (over z, y, x), tp: 2 (over core).
Axes of the slice: x: 2, y: 2, z: 4, core: 2. Of those that a mesh axis runs over, the one named last changes fastest.
Arguments:
- queries_small: bfloat16 [4096, 1024], P('sp', 'tp'), may hold values from -160 to 160
- queries_large: bfloat16 [4096, 1024], P('sp', 'tp'), may hold values from -160 to 160
- kv_small: bfloat16 [4096, 128], P('sp'), may hold values from -4 to 4
- kv_large: bfloat16 [4096, 256], P('sp'), may hold values from -4 to 4
- cum_small: float32 [16, 4096], P('tp', 'sp'), may hold values from -514 to 0, as said below
- cum_large: float32 [8, 4096], P('tp', 'sp'), may hold values from -514 to 0, as said below
- residual: bfloat16 [4096, 2048], P(('sp', 'tp')), may hold values from -6 to 6
- out_small: bfloat16 [1024, 2048], replicated, may hold values from -0.125 to 0.125
- out_large: bfloat16 [1024, 2048], replicated, may hold values from -0.125 to 0.125
- gain_mix: float32 [2048], replicated, may hold values from 0.1 to 1.9
- gain_route: float32 [2048], replicated, may hold values from 0.1 to 1.9
- gain_blend: float32 [2048], replicated, may hold values from 0.1 to 1.9
- w_gate: bfloat16 [32, 2048, 1024], P(('sp', 'tp')), may hold values from -0.125 to 0.125
- w_up: bfloat16 [32, 2048, 1024], P(('sp', 'tp')), may hold values from -0.125 to 0.125
- w_down: bfloat16 [32, 1024, 2048], P(('sp', 'tp')), may hold values from -0.1875 to 0.1875
- route: int32 [2, 4096], P(None, ('sp', 'tp')), may hold values from 0 to 31, as said below
- route_bias: float32 [4096], P(('sp', 'tp')), may hold values from -6 to 6
Outputs:
- result: bfloat16 [4096, 2048], P(('sp', 'tp'))
Inputs may be any that keep to these rules, and one draw needn't show every extreme that they name: `cum_small`: each row is non-increasing along positions. `cum_large`: each row is non-increasing along positions. route[0, t] and route[1, t] are different experts of the same group of 8 consecutive experts. Among the 128 positions of one device (aligned blocks), no expert is named by more than 16 of them; in every draw all experts of one group are named by exactly 16 positions of every device. Within one device's positions the loads of the experts of one group differ by at most 2.
All inputs are finite; a program needn't handle non-finite values.
Results may differ from a plain program's by a relative error of at most 0.014.
Values may be sent and summed in bfloat16 or wider, within the bound.
A program may use at most 128 MiB of HBM per device.

v0:
```python
import functools
import math

import jax
import jax.numpy as jnp
from jax import lax
from jax.experimental import pallas as pl
from jax.experimental.pallas import tpu as pltpu
from jax.sharding import PartitionSpec as P

norm_eps = 1e-06
far_score = -1e30
log2e = math.log2(math.e)
MESH = pl.DeviceIdType.MESH


def rms_scale(values, gain_row):
    return (
        values * lax.rsqrt(jnp.mean(values * values, axis=-1, keepdims=True) + norm_eps) * gain_row
    )


def mesh_shape(mesh):
    coords = [tuple(device.coords) for device in mesh.devices.reshape(-1)]
    return tuple(1 + max(c[axis] for c in coords) - min(c[axis] for c in coords) for axis in (2, 1, 0))


def gather_kernel(dims, kv_ref, cum_ref, kv_all, cum_all, send_kv, send_cum, send_core, recv_kv, recv_cum, recv_core, own_sem):
    depth, rows_y, rows_x = dims
    plane = rows_y * rows_x
    me = lax.axis_index("sp")
    core = lax.axis_index("tp")
    mine_z = me // plane
    mine_y = me % plane // rows_x
    mine_x = me % rows_x
    half = kv_ref.shape[0] // 2
    barrier = pltpu.get_barrier_semaphore()
    peers = 0
    for step in range(1, depth):
        target = (mine_z + step) % depth * plane + me % plane
        pl.semaphore_signal(barrier, inc=1, device_id=(target, core), device_id_type=MESH)
        peers += 1
    for step in range(1, rows_y):
        target = mine_z * plane + (mine_y + step) % rows_y * rows_x + mine_x
        pl.semaphore_signal(barrier, inc=1, device_id=(target, core), device_id_type=MESH)
        peers += 1
    for step in range(1, rows_x):
        target = mine_z * plane + mine_y * rows_x + (mine_x + step) % rows_x
        pl.semaphore_signal(barrier, inc=1, device_id=(target, core), device_id_type=MESH)
        peers += 1
    pl.semaphore_signal(barrier, inc=1, device_id=(me, 1 - core), device_id_type=MESH)
    own_kv = pltpu.make_async_copy(kv_ref, kv_all.at[me], own_sem.at[0])
    own_cum = pltpu.make_async_copy(cum_ref, cum_all.at[me], own_sem.at[1])
    own_kv.start()
    own_cum.start()
    own_kv.wait()
    own_cum.wait()
    pl.semaphore_wait(barrier, peers + 1)

    def copies(shard, target, slot):
        part = kv_all.at[shard, pl.ds(core * half, half)]
        return (
            pltpu.make_async_remote_copy(
                src_ref=part, dst_ref=part, send_sem=send_kv.at[slot], recv_sem=recv_kv.at[shard],
                device_id=(target, core), device_id_type=MESH),
            pltpu.make_async_remote_copy(
                src_ref=cum_all.at[shard], dst_ref=cum_all.at[shard], send_sem=send_cum.at[slot],
                recv_sem=recv_cum.at[shard], device_id=(target, core), device_id_type=MESH),
        )

    def across(shard):
        part = kv_all.at[shard, pl.ds(core * half, half)]
        return pltpu.make_async_remote_copy(
            src_ref=part, dst_ref=part, send_sem=send_core.at[shard], recv_sem=recv_core.at[shard],
            device_id=(me, 1 - core), device_id_type=MESH)

    def arrived(shard):
        for copy in copies(shard, me, 0):
            copy.wait_recv()

    def other_half(shard):
        part = kv_all.at[shard, pl.ds((1 - core) * half, half)]
        return pltpu.make_async_remote_copy(
            src_ref=part, dst_ref=part, send_sem=send_core.at[shard], recv_sem=recv_core.at[shard],
            device_id=(me, 1 - core), device_id_type=MESH)

    def route(first_axis):
        size_a, size_b = (rows_y, rows_x) if first_axis == "y" else (rows_x, rows_y)
        here_a, here_b = (mine_y, mine_x) if first_axis == "y" else (mine_x, mine_y)

        def index(z, a, b):
            return z * plane + (a * rows_x + b if first_axis == "y" else b * rows_x + a)

        sends = []
        slot = 0
        for step in range(1, depth):
            sends.append((mine_z + step < depth, index(mine_z, here_a, here_b), index(mine_z + step, here_a, here_b), slot))
            slot += 1

        def start(items):
            for _, shard, target, number in items:
                for copy in copies(shard, target, number):
                    copy.start()

        for item in sends:
            pl.when(item[0])(functools.partial(start, [item]))
        for behind in range(depth):
            z = mine_z - behind
            items = []
            shard = index(z, here_a, here_b)
            for step in range(1, size_a):
                items.append((z >= 0, shard, index(mine_z, (here_a + step) % size_a, here_b), slot))
                slot += 1
            for step in range(1, size_b):
                items.append((z >= 0, shard, index(mine_z, here_a, (here_b + step) % size_b), slot))
                slot += 1
            sends += items

            def forward(items=items, shard=shard, behind=behind):
                if behind:
                    arrived(shard)
                start(items)
                if behind:
                    across(shard).start()

            pl.when(z >= 0)(forward)
        for behind in range(depth):
            z = mine_z - behind
            for step_a in range(1, size_a):
                shard = index(z, (here_a + size_a - step_a) % size_a, here_b)
                items = []
                for step in range(1, size_b):
                    items.append((z >= 0, shard, index(mine_z, here_a, (here_b + step) % size_b), slot))
                    slot += 1
                sends += items

                def relay(items=items, shard=shard):
                    arrived(shard)
                    start(items)
                    across(shard).start()

                pl.when(z >= 0)(relay)
        for behind in range(depth):
            z = mine_z - behind
            for step_b in range(1, size_b):
                for step_a in range(size_a):
                    shard = index(z, (here_a + size_a - step_a) % size_a, (here_b + size_b - step_b) % size_b)

                    def last(shard=shard):
                        arrived(shard)
                        across(shard).start()

                    pl.when(z >= 0)(last)
        for behind in range(depth):
            z = mine_z - behind

            def settle(z=z):
                for place in range(plane):

                    def finish_half(shard=z * plane + place):
                        other_half(shard).wait_recv()
                        across(shard).wait_send()

                    pl.when(z * plane + place != me)(finish_half)

            pl.when(z >= 0)(settle)
        for item in sends:

            def sent(item=item):
                for copy in copies(item[1], item[2], item[3]):
                    copy.wait_send()

            pl.when(item[0])(sent)

    pl.when(core == 0)(functools.partial(route, "y"))
    pl.when(core == 1)(functools.partial(route, "x"))


def gather_keys(dims, kv, cum):
    shards = lax.axis_size("sp")
    depth, rows_y, rows_x = dims
    slots = depth - 1 + depth * (rows_y + rows_x - 2) + depth * (rows_y - 1) * (rows_x - 1)
    dma = pltpu.SemaphoreType.DMA
    return pl.pallas_call(
        functools.partial(gather_kernel, dims),
        out_shape=(
            jax.ShapeDtypeStruct((shards,) + kv.shape, kv.dtype),
            jax.ShapeDtypeStruct((shards,) + cum.shape, cum.dtype),
        ),
        in_specs=[pl.BlockSpec(memory_space=pltpu.VMEM)] * 2,
        out_specs=(pl.BlockSpec(memory_space=pltpu.VMEM),) * 2,
        scratch_shapes=[
            dma((slots,)), dma((slots,)), dma((shards,)), dma((shards,)), dma((shards,)), dma((shards,)), dma((2,)),
        ],
        compiler_params=pltpu.CompilerParams(collective_id=0, has_side_effects=True),
        name="gather_keys",
    )(kv, cum)


def attend_kernel(head_shape, group, q_small, q_large, kv_all, cum_all, o_small, o_large, qs, ql, top, total, acc_s, acc_l):
    heads_small, heads_large, size_small, size_large = head_shape
    me = lax.axis_index("sp")
    tokens = q_small.shape[0]
    width = group * tokens
    for h in range(heads_small):
        qs[h] = q_small[:, h * size_small:(h + 1) * size_small]
    for h in range(heads_large):
        ql[h] = q_large[:, h * size_large:(h + 1) * size_large]
    top[...] = jnp.full_like(top, far_score)
    total[...] = jnp.zeros_like(total)
    acc_s[...] = jnp.zeros_like(acc_s)
    acc_l[...] = jnp.zeros_like(acc_l)

    def block(number, masked):
        first = number * group

        def run(heads, base, q_ref, acc_ref, column, size):
            scale = size ** (-0.5) * log2e

            def one(h):
                keys = kv_all[pl.ds(first, group), :, column:column + size].reshape(width, size)
                values = kv_all[pl.ds(first, group), :, column + size:column + 2 * size].reshape(width, size)
                gates = jnp.concatenate(
                    [cum_all[first + j, pl.ds(base + h, 1), :] for j in range(group)], axis=1
                ) * log2e
                scores = lax.dot_general(
                    q_ref[h], keys, (((1,), (1,)), ((), ())), preferred_element_type=jnp.float32
                ) * scale - gates
                if masked:
                    key_pos = lax.broadcasted_iota(jnp.int32, (tokens, width), 1) + first * tokens
                    query_pos = lax.broadcasted_iota(jnp.int32, (tokens, width), 0) + me * tokens
                    scores = jnp.where(key_pos <= query_pos, scores, far_score)
                before = top[base + h]
                newest = jnp.maximum(before, jnp.max(scores, axis=-1, keepdims=True))
                factor = jnp.exp2(before - newest)
                weights = jnp.exp2(scores - newest[:, :1])
                partial_sum = weights[:, :128]
                for j in range(1, width // 128):
                    partial_sum = partial_sum + weights[:, j * 128:(j + 1) * 128]
                product = jnp.dot(
                    weights.astype(jnp.bfloat16), values, preferred_element_type=jnp.float32
                )
                return (
                    newest,
                    total[base + h] * factor + partial_sum,
                    acc_ref[h] * factor[:, :size] + product,
                )

            together = math.gcd(heads, 2)

            def several(number, _):
                found = [one(number * together + j) for j in range(together)]
                for j in range(together):
                    h = number * together + j
                    top[base + h], total[base + h], acc_ref[h] = found[j]
                return 0

            lax.fori_loop(0, heads // together, several, 0)

        run(heads_small, 0, qs, acc_s, 0, size_small)
        run(heads_large, heads_small, ql, acc_l, 2 * size_small, size_large)

    last = me // group

    def whole(number, _):
        block(number, False)
        return 0

    lax.fori_loop(0, last, whole, 0)
    block(last, True)
    for h in range(heads_small):
        o_small[:, h * size_small:(h + 1) * size_small] = (
            acc_s[h] / jnp.sum(total[h], axis=-1, keepdims=True)
        ).astype(o_small.dtype)
    for h in range(heads_large):
        o_large[:, h * size_large:(h + 1) * size_large] = (
            acc_l[h] / jnp.sum(total[heads_small + h], axis=-1, keepdims=True)
        ).astype(o_large.dtype)


def attend(queries_small, queries_large, kv_all, cum_all, head_shape, group):
    heads_small, heads_large, size_small, size_large = head_shape
    tokens = queries_small.shape[0]
    heads = heads_small + heads_large
    return pl.pallas_call(
        functools.partial(attend_kernel, head_shape, group),
        out_shape=(
            jax.ShapeDtypeStruct(queries_small.shape, jnp.bfloat16),
            jax.ShapeDtypeStruct(queries_large.shape, jnp.bfloat16),
        ),
        in_specs=[pl.BlockSpec(memory_space=pltpu.VMEM)] * 4,
        out_specs=(pl.BlockSpec(memory_space=pltpu.VMEM),) * 2,
        scratch_shapes=[
            pltpu.VMEM((heads_small, tokens, size_small), jnp.bfloat16),
            pltpu.VMEM((heads_large, tokens, size_large), jnp.bfloat16),
            pltpu.VMEM((heads, tokens, 128), jnp.float32),
            pltpu.VMEM((heads, tokens, 128), jnp.float32),
            pltpu.VMEM((heads_small, tokens, size_small), jnp.float32),
            pltpu.VMEM((heads_large, tokens, size_large), jnp.float32),
        ],
        compiler_params=pltpu.CompilerParams(vmem_limit_bytes=56 * 1024 * 1024),
        name="attend",
    )(queries_small, queries_large, kv_all, cum_all)


def greet(depth, plane, cores, me, core):
    barrier = pltpu.get_barrier_semaphore()
    lanes = plane * cores
    here = me % plane * cores + core
    for step in range(1, depth):
        target = (me // plane + step) % depth * plane + me % plane
        pl.semaphore_signal(barrier, inc=1, device_id=(target, core), device_id_type=MESH)
    for step in range(1, lanes):
        other = (here + step) % lanes
        target = me // plane * plane + other // cores
        pl.semaphore_signal(barrier, inc=1, device_id=(target, other % cores), device_id_type=MESH)
    pl.semaphore_wait(barrier, depth - 1 + lanes - 1)


def distances(depth):
    found = [0]
    for step in range(1, depth):
        found += [step, -step]
    return found


def dispatch_kernel(depth, cores, rows_ref, meta_ref, received, metas, in_rows, stage, send_rows, send_meta, recv_rows, recv_meta, send_block, recv_block, own_sem):
    me = lax.axis_index("sp")
    core = lax.axis_index("tp")
    _, lanes, capacity, columns = stage.shape
    plane = lanes // cores
    slots = rows_ref.shape[1]
    mine = me // plane
    here = me % plane * cores + core
    own_rows = pltpu.make_async_copy(rows_ref.at[mine], in_rows.at[mine], own_sem.at[0, 0])
    own_meta = pltpu.make_async_copy(meta_ref.at[mine], metas.at[mine], own_sem.at[0, 1])
    own_rows.start()
    own_meta.start()
    greet(depth, plane, cores, me, core)

    def along(other):
        target = (other * plane + me % plane, core)
        return (
            pltpu.make_async_remote_copy(
                src_ref=rows_ref.at[other], dst_ref=in_rows.at[mine], send_sem=send_rows.at[other],
                recv_sem=recv_rows.at[mine], device_id=target, device_id_type=MESH),
            pltpu.make_async_remote_copy(
                src_ref=meta_ref.at[other], dst_ref=metas.at[mine], send_sem=send_meta.at[other],
                recv_sem=recv_meta.at[mine], device_id=target, device_id_type=MESH),
        )

    def incoming(other):
        target = (other * plane + me % plane, core)
        return (
            pltpu.make_async_remote_copy(
                src_ref=rows_ref.at[other], dst_ref=in_rows.at[other], send_sem=send_rows.at[other],
                recv_sem=recv_rows.at[other], device_id=target, device_id_type=MESH),
            pltpu.make_async_remote_copy(
                src_ref=meta_ref.at[other], dst_ref=metas.at[other], send_sem=send_meta.at[other],
                recv_sem=recv_meta.at[other], device_id=target, device_id_type=MESH),
        )

    def block(source, other, slot_of):
        return pltpu.make_async_remote_copy(
            src_ref=stage.at[source, other], dst_ref=received.at[source * lanes + slot_of],
            send_sem=send_block.at[source, other], recv_sem=recv_block.at[source, slot_of],
            device_id=(mine * plane + other // cores, other % cores), device_id_type=MESH)

    def keep(source):
        return pltpu.make_async_copy(
            stage.at[source, here], received.at[source * lanes + here], own_sem.at[1, source])

    steps = distances(depth)
    for step in steps[1:]:
        other = mine + step

        def launch(other=other):
            for copy in along(other):
                copy.start()

        pl.when((other >= 0) & (other < depth))(launch)
    own_rows.wait()
    own_meta.wait()
    for step in steps:
        other = mine + step

        def expand(other=other, step=step):
            if step:
                for copy in incoming(other):
                    copy.wait_recv()
            wanted = lax.broadcasted_iota(jnp.int32, (lanes * capacity, slots), 0).astype(jnp.float32) + 1.0
            first = metas[other, 0:1, :slots]
            second = metas[other, 1:2, :slots]
            table = jnp.where((wanted == first) | (wanted == second), 1.0, 0.0).astype(jnp.bfloat16)
            spread = jnp.dot(table, in_rows[other], preferred_element_type=jnp.float32)
            for lane in range(lanes):
                stage[other, lane] = spread[lane * capacity:(lane + 1) * capacity].astype(jnp.bfloat16)
            for move in range(1, lanes):
                block(other, (here + move) % lanes, here).start()
            keep(other).start()

        pl.when((other >= 0) & (other < depth))(expand)
    for source in range(depth):
        keep(source).wait()
        for move in range(1, lanes):
            block(source, (here + move) % lanes, (here + move) % lanes).wait_recv()
            block(source, (here + move) % lanes, here).wait_send()
    for step in steps[1:]:
        other = mine + step

        def sent(other=other):
            for copy in along(other):
                copy.wait_send()

        pl.when((other >= 0) & (other < depth))(sent)


def dispatch(rows, meta, lanes, cores, capacity):
    depth, slots, columns = rows.shape
    dma = pltpu.SemaphoreType.DMA
    vmem = pl.BlockSpec(memory_space=pltpu.VMEM)
    return pl.pallas_call(
        functools.partial(dispatch_kernel, depth, cores),
        out_shape=(
            jax.ShapeDtypeStruct((depth * lanes, capacity, columns), rows.dtype),
            jax.ShapeDtypeStruct(meta.shape, meta.dtype),
        ),
        in_specs=[vmem] * 2,
        out_specs=(vmem,) * 2,
        scratch_shapes=[
            pltpu.VMEM(rows.shape, rows.dtype),
            pltpu.VMEM((depth, lanes, capacity, columns), rows.dtype),
            dma((depth,)), dma((depth,)), dma((depth,)), dma((depth,)),
            dma((depth, lanes)), dma((depth, lanes)), dma((2, max(depth, 2))),
        ],
        compiler_params=pltpu.CompilerParams(
            collective_id=1, has_side_effects=True, vmem_limit_bytes=48 * 1024 * 1024),
        name="dispatch_rows",
    )(rows, meta)


def return_kernel(depth, cores, outs, metas, final, back, stage, send_block, recv_block, send_rows, recv_rows, own_sem):
    me = lax.axis_index("sp")
    core = lax.axis_index("tp")
    _, lanes, capacity, columns = back.shape
    plane = lanes // cores
    slots = final.shape[1]
    mine = me // plane
    here = me % plane * cores + core
    greet(depth, plane, cores, me, core)

    def block(source, other, slot_of):
        return pltpu.make_async_remote_copy(
            src_ref=outs.at[source * lanes + other], dst_ref=back.at[source, slot_of],
            send_sem=send_block.at[source, other], recv_sem=recv_block.at[source, slot_of],
            device_id=(mine * plane + other // cores, other % cores), device_id_type=MESH)

    def keep(source):
        return pltpu.make_async_copy(
            outs.at[source * lanes + here], back.at[source, here], own_sem.at[source])

    def along(other, slot_of):
        return pltpu.make_async_remote_copy(
            src_ref=stage.at[other], dst_ref=final.at[slot_of], send_sem=send_rows.at[other],
            recv_sem=recv_rows.at[slot_of], device_id=(other * plane + me % plane, core), device_id_type=MESH)

    steps = distances(depth)[::-1]
    for step in steps:
        other = mine + step

        def launch(other=other):
            for move in range(1, lanes):
                block(other, (here + move) % lanes, here).start()
            keep(other).start()

        pl.when((other >= 0) & (other < depth))(launch)
    for step in steps:
        other = mine + step

        def combine(other=other, step=step):
            keep(other).wait()
            for move in range(1, lanes):
                block(other, (here + move) % lanes, (here + move) % lanes).wait_recv()
            count = lanes * capacity
            width = metas.shape[2]
            wanted = lax.broadcasted_iota(jnp.int32, (count, width), 0).astype(jnp.float32) + 1.0
            weights = jnp.where(wanted == metas[other, 0:1, :], metas[other, 2:3, :], 0.0)
            weights = weights + jnp.where(wanted == metas[other, 1:2, :], metas[other, 3:4, :], 0.0)
            weights = weights.T[:slots]
            high = weights.astype(jnp.bfloat16)
            low = (weights - high.astype(jnp.float32)).astype(jnp.bfloat16)
            if capacity % 16:
                picked = jnp.concatenate(
                    [back[other, lane].astype(jnp.float32) for lane in range(lanes)], axis=0
                ).astype(jnp.bfloat16)
            else:
                picked = back[other].reshape(count, columns)
            mixed = jnp.dot(high, picked, preferred_element_type=jnp.float32) + jnp.dot(
                low, picked, preferred_element_type=jnp.float32)
            if step:
                stage[other] = mixed.astype(stage.dtype)
                along(other, mine).start()
            else:
                final[other] = mixed.astype(final.dtype)

        pl.when((other >= 0) & (other < depth))(combine)
    for step in steps:
        other = mine + step

        def settle(other=other, step=step):
            for move in range(1, lanes):
                block(other, (here + move) % lanes, here).wait_send()
            if step:
                along(other, other).wait_recv()
                along(other, mine).wait_send()

        pl.when((other >= 0) & (other < depth))(settle)


def give_back(outs, metas, lanes, cores, slots):
    depth = metas.shape[0]
    _, capacity, columns = outs.shape
    dma = pltpu.SemaphoreType.DMA
    vmem = pl.BlockSpec(memory_space=pltpu.VMEM)
    return pl.pallas_call(
        functools.partial(return_kernel, depth, cores),
        out_shape=jax.ShapeDtypeStruct((depth, slots, columns), outs.dtype),
        in_specs=[vmem] * 2,
        out_specs=vmem,
        scratch_shapes=[
            pltpu.VMEM((depth, lanes, capacity, columns), outs.dtype),
            pltpu.VMEM((depth, slots, columns), outs.dtype),
            dma((depth, lanes)), dma((depth, lanes)), dma((depth,)), dma((depth,)), dma((depth,)),
        ],
        compiler_params=pltpu.CompilerParams(
            collective_id=2, has_side_effects=True, vmem_limit_bytes=48 * 1024 * 1024),
        name="return_rows",
    )(outs, metas)


def earlier_same(ids):
    order = jnp.arange(ids.shape[0], dtype=jnp.int32)
    same = (ids[:, None] == ids[None, :]) & (order[None, :] < order[:, None])
    return jnp.sum(same.astype(jnp.int32), axis=1)


def on_device(
    dims,
    queries_small,
    queries_large,
    kv_small,
    kv_large,
    cum_small,
    cum_large,
    residual,
    out_small,
    out_large,
    gain_mix,
    gain_route,
    gain_blend,
    w_gate,
    w_up,
    w_down,
    route,
    route_bias,
):
    tokens_here = queries_small.shape[0]
    heads_small = cum_small.shape[0]
    heads_large = cum_large.shape[0]
    size_small = kv_small.shape[1] // 2
    size_large = kv_large.shape[1] // 2
    kv_all, cum_all = gather_keys(
        dims,
        jnp.concatenate([kv_small, kv_large], axis=1),
        jnp.concatenate([cum_small, cum_large], axis=0),
    )
    group = math.gcd(dims[1] * dims[2], 4)
    attn_small, attn_large = attend(
        queries_small,
        queries_large,
        kv_all,
        cum_all,
        (heads_small, heads_large, size_small, size_large),
        group,
    )
    row_count = tokens_here // lax.axis_size("tp")
    whole_small, whole_large = (
        lax.all_to_all(attn_small, "tp", split_axis=0, concat_axis=1, tiled=True),
        lax.all_to_all(attn_large, "tp", split_axis=0, concat_axis=1, tiled=True),
    )
    mixer_out = jnp.dot(whole_small, out_small, preferred_element_type=jnp.float32) + jnp.dot(
        whole_large, out_large, preferred_element_type=jnp.float32
    )
    mixed = (residual.astype(jnp.float32) + rms_scale(mixer_out, gain_mix)).astype(jnp.bfloat16)
    routed = rms_scale(mixed.astype(jnp.float32), gain_route).astype(jnp.bfloat16)
    experts = lax.axis_size(("sp", "tp"))
    cores = lax.axis_size("tp")
    depth = dims[0]
    lanes = experts // depth
    capacity = 4 * row_count // experts
    slots = capacity * lanes // 2
    group_ids = route[0] // lanes
    row_slots = group_ids * slots + earlier_same(group_ids)
    row_table = row_slots[None, :] == jnp.arange(depth * slots, dtype=jnp.int32)[:, None]
    flat_ids = route.reshape(2 * row_count)
    places = (flat_ids % lanes * capacity + earlier_same(flat_ids) + 1).astype(jnp.float32)
    facts = jnp.stack(
        [places[:row_count], places[row_count:], jax.nn.sigmoid(route_bias), jax.nn.sigmoid(-route_bias)]
    )
    meta = jnp.sum(jnp.where(row_table[None], facts[:, None, :], 0.0), axis=2)
    meta = meta.reshape(4, depth, slots).transpose(1, 0, 2)
    meta = jnp.pad(meta, ((0, 0), (0, 4), (0, -slots % 128)))
    outgoing = jnp.dot(
        row_table.astype(jnp.bfloat16), routed, preferred_element_type=jnp.float32
    ).astype(jnp.bfloat16)
    received, metas = dispatch(
        outgoing.reshape(depth, slots, routed.shape[1]), meta, lanes, cores, capacity
    )
    row_total = received.shape[0] * received.shape[1]
    expert_rows = received.reshape(row_total, received.shape[2])
    gate_pre = jnp.dot(expert_rows, w_gate[0], preferred_element_type=jnp.float32)
    up_pre = jnp.dot(expert_rows, w_up[0], preferred_element_type=jnp.float32)
    hidden = (jax.nn.silu(gate_pre) * up_pre).astype(jnp.bfloat16)
    expert_out = jnp.dot(hidden, w_down[0], preferred_element_type=jnp.float32).astype(jnp.bfloat16)
    returned = give_back(expert_out.reshape(received.shape), metas, lanes, cores, slots)
    blended = lax.dot_general(
        row_table.astype(jnp.bfloat16),
        returned.reshape(depth * slots, routed.shape[1]),
        (((0,), (0,)), ((), ())),
        preferred_element_type=jnp.float32,
    )
    return (mixed.astype(jnp.float32) + rms_scale(blended, gain_blend)).astype(jnp.bfloat16)


def solution(mesh):
    in_specs = (
        P("sp", "tp"),
        P("sp", "tp"),
        P("sp", None),
        P("sp", None),
        P("tp", "sp"),
        P("tp", "sp"),
        P(("sp", "tp"), None),
        P(),
        P(),
        P(),
        P(),
        P(),
        P(("sp", "tp"), None, None),
        P(("sp", "tp"), None, None),
        P(("sp", "tp"), None, None),
        P(None, ("sp", "tp")),
        P(("sp", "tp")),
    )
    out_specs = P(("sp", "tp"), None)
    return jax.shard_map(
        functools.partial(on_device, mesh_shape(mesh)), mesh=mesh, in_specs=in_specs, out_specs=out_specs, check_vma=False
    )
```

profile of v0, /device:TPU:9, one launch (start us, length us, event | category | flops | bytes accessed | tf_op | source)
XLA Modules:
  0.0 179.3 jit_solution(16468846003908605664)
XLA Ops:
  0.0 1.3 pad_maximum_fusion.1.cum_ref
  1.3 1.6 pad_maximum_fusion.kv_ref
  3.0 22.4 %gather_keys.1 = (bf16[16,256,384]{2,1,0:T(8,128)(2,1)}, f32[16,12,256]{2,1,0:T(8,128)}) custom-call(bf16[256,384]{1,0:T(8,128)(2,1)} %pad_maximum_fusion.kv_ref, f32[12,256]{1,0:T(8,128)} %pad_maximum_fusion.1.cum_ref), custom_call_target="tpu_custom_call" | custom-call | tf_op jit(solution)/shard_map/gather_keys/pallas_call | solution.py:184
  25.4 20.9 %attend.1 = (bf16[256,512]{1,0:T(8,128)(2,1)}, bf16[256,512]{1,0:T(8,128)(2,1)}) custom-call(bf16[256,512]{1,0:T(8,128)(2,1)} %q_small.1, bf16[256,512]{1,0:T(8,128)(2,1)} %q_large.1, bf16[16,256,384]{2,1,0:T(8,128)(2,1)} %get-tuple-element.11.kv_all, f32[16,12,256]{2,1,0:T(8,128)} %get-tuple-element.12.cum_all), custom_call_target="tpu_custom_call" | custom-call | tf_op jit(solution)/shard_map/attend/pallas_call | solution.py:285
  46.3 1.8 copy.21
  48.1 3.6 %all-to-all-start = ((bf16[2,128,512]{1,2,0:T(8,128)(2,1)}), bf16[2,128,512]{1,2,0:T(8,128)(2,1)S(1)}, u32[]{:S(2)}, u32[]{:S(2)}) async-start(bf16[2,128,512]{1,2,0:T(8,128)(2,1)} %copy.21), calls=%async_computation | async-start | bytes 524288 | tf_op jit(solution)/shard_map/all_to_all | solution.py:588
  51.7 0.2 convert_reduce_fusion.1
  51.9 0.2 convert_reduce_fusion
  52.2 0.2 select_reduce_fusion
  52.4 0.1 reshape.107
  52.5 1.8 %copy.22 = bf16[2,128,512]{1,2,0:T(8,128)(2,1)} copy(bf16[2,128,512]{2,1,0:T(8,128)(2,1)} %bitcast.70) | data formatting | bytes 524288 | tf_op jit(solution)/shard_map/all_to_all | solution.py:589
  54.3 0.0 all-to-all-done
  54.3 3.5 %all-to-all-start.1 = ((bf16[2,128,512]{1,2,0:T(8,128)(2,1)}), bf16[2,128,512]{1,2,0:T(8,128)(2,1)S(1)}, u32[]{:S(2)}, u32[]{:S(2)}) async-start(bf16[2,128,512]{1,2,0:T(8,128)(2,1)} %copy.22), calls=%async_computation.1 | async-start | bytes 524288 | tf_op jit(solution)/shard_map/all_to_all | solution.py:589
  57.7 2.9 %fusion.30 = f32[128,2048]{1,0:T(8,128)S(1)} fusion(bf16[128,1024]{0,1:T(8,128)(2,1)S(1)} %bitcast.68, bf16[1024,2048]{1,0:T(8,128)(2,1)} %param.24), kind=kOutput, calls=%fused_computation.63 | convolution fusion | flops 536870912 | bytes 5505024 | tf_op jit(solution)/shard_map/dot_general | solution.py:591
  60.7 0.0 all-to-all-done.1
  60.7 0.0 copy-start.1
  60.7 0.0 copy-start.3
  60.7 0.0 copy-start.4
  60.7 3.1 %multiply_reduce_fusion.1 = (f32[128]{0:T(128)S(1)}, f32[128,2048]{1,0:T(8,128)S(1)}) fusion(f32[128,2048]{1,0:T(8,128)S(1)} %fusion.30, bf16[128,1024]{0,1:T(8,128)(2,1)S(1)} %bitcast.69, bf16[1024,2048]{1,0:T(8,128)(2,1)} %param.25), kind=kOutput, calls=%fused_computation.19 | convolution fusion | flops 537657216 | bytes 6554112 | tf_op jit(solution)/shard_map/dot_general | solution.py:591
  63.8 0.0 copy-start.7
  63.8 0.0 copy-done.1
  63.8 0.0 copy-done.3
  63.8 0.4 fusion.11
  64.2 0.5 convolution_convert_fusion
  64.7 52.7 %dispatch_rows.1 = (bf16[32,16,2048]{2,1,0:T(8,128)(2,1)S(1)}, f32[4,8,128]{2,1,0:T(8,128)S(1)}) custom-call(bf16[4,64,2048]{2,1,0:T(8,128)(2,1)S(1)} %bitcast.64, f32[4,8,128]{2,1,0:T(8,128)S(1)} %pad.4.meta_ref), custom_call_target="tpu_custom_call" | custom-call | tf_op jit(solution)/shard_map/dispatch_rows/pallas_call | solution.py:422
  117.4 1.3 copy-done
  118.7 3.7 %fusion.4 = f32[512,1024]{1,0:T(8,128)} fusion(bf16[512,2048]{1,0:T(8,128)(2,1)S(1)} %bitcast.66, bf16[1,2048,1024]{2,1,0:T(8,128)(2,1)S(1)} %copy-done.7), kind=kOutput, calls=%fused_computation.4 | convolution fusion | flops 2147483648 | bytes 8388608 | tf_op jit(solution)/shard_map/dot_general | solution.py:621
  122.4 9.2 %fusion.6 = bf16[512,2048]{1,0:T(8,128)(2,1)S(1)} fusion(bf16[1,1024,2048]{2,1,0:T(8,128)(2,1)} %param.31, f32[512,1024]{1,0:T(8,128)} %fusion.4, bf16[512,2048]{1,0:T(8,128)(2,1)} %bitcast.67, bf16[1,2048,1024]{2,1,0:T(8,128)(2,1)} %param.30), kind=kOutput, calls=%fused_computation.6 | convolution fusion | flops 4299161600 | bytes 14680064 | tf_op jit(solution)/shard_map/dot_general | solution.py:624
  131.6 0.0 copy-start.5
  131.6 46.1 %return_rows.1 = bf16[4,64,2048]{2,1,0:T(8,128)(2,1)S(1)} custom-call(bf16[32,16,2048]{2,1,0:T(8,128)(2,1)S(1)} %bitcast.65, f32[4,8,128]{2,1,0:T(8,128)S(1)} %get-tuple-element.16.metas), custom_call_target="tpu_custom_call" | custom-call | tf_op jit(solution)/shard_map/return_rows/pallas_call | solution.py:525
  177.8 0.4 multiply_reduce_fusion
  178.2 1.0 fusion.14
  (20 shorter events, 0.1 us)
Async XLA Ops:
  0.0 51.7 %copy-start.2 = (s32[2,128]{1,0:T(2,128)S(1)}, s32[2,128]{1,0:T(2,128)}, u32[]{:S(2)}) copy-start(s32[2,128]{1,0:T(2,128)} %param.32) | copy-start | bytes 3076
  0.0 52.1 %copy-start.6 = (f32[128]{0:T(128)S(1)}, f32[128]{0:T(128)}, u32[]{:S(2)}) copy-start(f32[128]{0:T(128)} %param.33) | copy-start | bytes 1540
  48.1 6.2 %all-to-all-start = ((bf16[2,128,512]{1,2,0:T(8,128)(2,1)}), bf16[2,128,512]{1,2,0:T(8,128)(2,1)S(1)}, u32[]{:S(2)}, u32[]{:S(2)}) async-start(bf16[2,128,512]{1,2,0:T(8,128)(2,1)} %copy.21), calls=%async_computation | async-start | bytes 524288 | tf_op jit(solution)/shard_map/all_to_all | solution.py:588
  54.3 6.4 %all-to-all-start.1 = ((bf16[2,128,512]{1,2,0:T(8,128)(2,1)}), bf16[2,128,512]{1,2,0:T(8,128)(2,1)S(1)}, u32[]{:S(2)}, u32[]{:S(2)}) async-start(bf16[2,128,512]{1,2,0:T(8,128)(2,1)} %copy.22), calls=%async_computation.1 | async-start | bytes 524288 | tf_op jit(solution)/shard_map/all_to_all | solution.py:589
  60.7 3.1 %copy-start.1 = (bf16[128,2048]{1,0:T(8,128)(2,1)S(1)}, bf16[128,2048]{1,0:T(8,128)(2,1)}, u32[]{:S(2)}) copy-start(bf16[128,2048]{1,0:T(8,128)(2,1)} %param.23) | copy-start | bytes 1572868
  60.7 3.1 %copy-start.3 = (f32[2048]{0:T(1024)S(1)}, f32[2048]{0:T(1024)}, u32[]{:S(2)}) copy-start(f32[2048]{0:T(1024)} %param.26) | copy-start | bytes 24580
  60.7 3.5 %copy-start.4 = (f32[2048]{0:T(1024)S(1)}, f32[2048]{0:T(1024)}, u32[]{:S(2)}) copy-start(f32[2048]{0:T(1024)} %param.27) | copy-start | bytes 24580
  63.8 54.9 %copy-start.7 = (bf16[1,2048,1024]{2,1,0:T(8,128)(2,1)S(1)}, bf16[1,2048,1024]{2,1,0:T(8,128)(2,1)}, u32[]{:S(2)}) copy-start(bf16[1,2048,1024]{2,1,0:T(8,128)(2,1)} %param.29) | copy-start | bytes 12582916
  117.4 1.3 copy-start
  131.6 46.6 %copy-start.5 = (f32[2048]{0:T(1024)S(1)}, f32[2048]{0:T(1024)}, u32[]{:S(2)}) copy-start(f32[2048]{0:T(1024)} %param.28) | copy-start | bytes 24580
where the time goes:
time: 180 us; the launch traced here: 179 us
  Pallas kernels  142 us (79%)
  matrix products  19.8 us (11%)
  starting transfers between devices  7.05 us (4%)
  other arithmetic  5.04 us (3%)
  local copies, waits for them, and re-layouts  5 us (3%)
    pallas_call x1, Pallas kernels, dispatch(): pl.pallas_call(functools.partial(dispatch_kernel, depth, cores), out_shap...  52.7 us
    pallas_call x1, Pallas kernels, give_back(): pl.pallas_call(functools.partial(return_kernel, depth, cores), out_shape=...  46.1 us
    pallas_call x1, Pallas kernels, gather_keys(): pl.pallas_call(functools.partial(gather_kernel, dims), out_shape=(jax.Sha...  22.4 us
    pallas_call x1, Pallas kernels, attend(): pl.pallas_call(functools.partial(attend_kernel, head_shape, group), out_s...  20.9 us
    dot_general x1, matrix products, on_device(): jnp.dot(hidden, w_down[0], preferred_element_type=jnp.float32)  9.23 us
    dot_general x1, matrix products, on_device(): jnp.dot(expert_rows, w_gate[0], preferred_element_type=jnp.float32)  3.69 us
  transfers between devices with their start and end apart: 2, of which 0 were waited for; matrix products, arithmetic and copies ran while one was open for 3% of the time, Pallas kernels for 0%

commit v1 on v0

--- a/solution.py
+++ b/solution.py
@@ -25,7 +25,26 @@
     return tuple(1 + max(c[axis] for c in coords) - min(c[axis] for c in coords) for axis in (2, 1, 0))
 
 
-def gather_kernel(dims, kv_ref, cum_ref, kv_all, cum_all, send_kv, send_cum, send_core, recv_kv, recv_cum, recv_core, own_sem):
+def bf16_pieces(values):
+    high = values.astype(jnp.bfloat16)
+    rest = values - high.astype(jnp.float32)
+    middle = rest.astype(jnp.bfloat16)
+    low = (rest - middle.astype(jnp.float32)).astype(jnp.bfloat16)
+    return [high.astype(jnp.float32), middle.astype(jnp.float32), low.astype(jnp.float32)]
+
+
+def round_up(value, unit):
+    return -(-value // unit) * unit
+
+
+def mix_kernel(
+    dims, head_shape,
+    q_small, q_large, kv_small, kv_large, cum_small, cum_large, residual, gain_mix, gain_route, out_small, out_large,
+    mixed_ref, routed_ref,
+    table, cums, qs, ql, top, total, acc_s, acc_l, stage, whole, weights, mixer,
+    send_far, send_near, send_core, recv_kv, recv_cum, recv_core, swap_send, swap_recv, load_sem,
+):
+    heads_small, heads_large, size_small, size_large = head_shape
     depth, rows_y, rows_x = dims
     plane = rows_y * rows_x
     me = lax.axis_index("sp")
@@ -33,274 +52,362 @@
     mine_z = me // plane
     mine_y = me % plane // rows_x
     mine_x = me % rows_x
-    half = kv_ref.shape[0] // 2
+    tokens = q_small.shape[0]
+    heads = heads_small + heads_large
+    extra_s = round_up(3 * heads_small, 32)
+    extra_l = round_up(3 * heads_large, 16)
+    wire = 2 * size_small + 2 * size_large
+    half = wire // 2
+    small_v = extra_s + size_small
+    large_v = small_v + size_small
+    large_k = large_v + size_large
+    gate_l = extra_s + wire
+
+    loads = (
+        pltpu.make_async_copy(out_small, weights.at[pl.ds(0, out_small.shape[0])], load_sem.at[0]),
+        pltpu.make_async_copy(
+            out_large, weights.at[pl.ds(out_small.shape[0], out_large.shape[0])], load_sem.at[1]),
+    )
+    for load in loads:
+        load.start()
     barrier = pltpu.get_barrier_semaphore()
-    peers = 0
     for step in range(1, depth):
         target = (mine_z + step) % depth * plane + me % plane
         pl.semaphore_signal(barrier, inc=1, device_id=(target, core), device_id_type=MESH)
-        peers += 1
     for step in range(1, rows_y):
         target = mine_z * plane + (mine_y + step) % rows_y * rows_x + mine_x
         pl.semaphore_signal(barrier, inc=1, device_id=(target, core), device_id_type=MESH)
-        peers += 1
     for step in range(1, rows_x):
         target = mine_z * plane + mine_y * rows_x + (mine_x + step) % rows_x
         pl.semaphore_signal(barrier, inc=1, device_id=(target, core), device_id_type=MESH)
-        peers += 1
     pl.semaphore_signal(barrier, inc=1, device_id=(me, 1 - core), device_id_type=MESH)
-    own_kv = pltpu.make_async_copy(kv_ref, kv_all.at[me], own_sem.at[0])
-    own_cum = pltpu.make_async_copy(cum_ref, cum_all.at[me], own_sem.at[1])
-    own_kv.start()
-    own_cum.start()
-    own_kv.wait()
-    own_cum.wait()
-    pl.semaphore_wait(barrier, peers + 1)
-
-    def copies(shard, target, slot):
-        part = kv_all.at[shard, pl.ds(core * half, half)]
+
+    def turned(block):
+        width = block.shape[1]
+        eye = jnp.where(
+            lax.broadcasted_iota(jnp.int32, (width, width), 0) == lax.broadcasted_iota(jnp.int32, (width, width), 1),
+            1.0, 0.0).astype(jnp.bfloat16)
+        return lax.dot_general(
+            eye, block, (((1,), (1,)), ((), ())), preferred_element_type=jnp.float32).astype(jnp.bfloat16)
+
+    table[me, extra_s:large_v, :] = turned(kv_small[...])
+    table[me, large_k:gate_l, :] = turned(kv_large[:, :size_large])
+    table[me, large_v:large_k, :] = turned(kv_large[:, size_large:])
+    cums[me, :heads_small] = cum_small[...]
+    cums[me, heads_small:heads] = cum_large[...]
+
+    lanes_s = lax.broadcasted_iota(jnp.int32, (tokens, extra_s), 1)
+    lanes_l = lax.broadcasted_iota(jnp.int32, (tokens, extra_l), 1)
+    for h in range(heads_small):
+        picks = jnp.where((lanes_s % heads_small == h) & (lanes_s < 3 * heads_small), 1.0, 0.0)
+        qs[h] = jnp.concatenate(
+            [picks.astype(jnp.bfloat16), q_small[:, h * size_small:(h + 1) * size_small]], axis=1)
+    for h in range(heads_large):
+        picks = jnp.where((lanes_l % heads_large == h) & (lanes_l < 3 * heads_large), 1.0, 0.0)
+        ql[h] = jnp.concatenate(
+            [q_large[:, h * size_large:(h + 1) * size_large], picks.astype(jnp.bfloat16)], axis=1)
+    pl.semaphore_wait(barrier, depth - 1 + rows_y - 1 + rows_x - 1 + 1)
+
+    def place(behind, off_y, off_x):
+        return (mine_z - behind) * plane + (mine_y + off_y) % rows_y * rows_x + (mine_x + off_x) % rows_x
+
+    def copies(shard, target, sems):
+        part = table.at[shard, pl.ds(extra_s + core * half, half)]
         return (
             pltpu.make_async_remote_copy(
-                src_ref=part, dst_ref=part, send_sem=send_kv.at[slot], recv_sem=recv_kv.at[shard],
+                src_ref=part, dst_ref=part, send_sem=sems.at[0], recv_sem=recv_kv.at[shard],
                 device_id=(target, core), device_id_type=MESH),
             pltpu.make_async_remote_copy(
-                src_ref=cum_all.at[shard], dst_ref=cum_all.at[shard], send_sem=send_cum.at[slot],
+                src_ref=cums.at[shard], dst_ref=cums.at[shard], send_sem=sems.at[1],
                 recv_sem=recv_cum.at[shard], device_id=(target, core), device_id_type=MESH),
         )
 
-    def across(shard):
-        part = kv_all.at[shard, pl.ds(core * half, half)]
+    def start(shard, target, sems):
+        for copy in copies(shard, target, sems):
+            copy.start()
+
+    def across(shard, which):
+        part = table.at[shard, pl.ds(extra_s + which * half, half)]
         return pltpu.make_async_remote_copy(
             src_ref=part, dst_ref=part, send_sem=send_core.at[shard], recv_sem=recv_core.at[shard],
             device_id=(me, 1 - core), device_id_type=MESH)
 
     def arrived(shard):
-        for copy in copies(shard, me, 0):
+        for copy in copies(shard, me, send_far.at[0]):
             copy.wait_recv()
-
-    def other_half(shard):
-        part = kv_all.at[shard, pl.ds((1 - core) * half, half)]
-        return pltpu.make_async_remote_copy(
-            src_ref=part, dst_ref=part, send_sem=send_core.at[shard], recv_sem=recv_core.at[shard],
-            device_id=(me, 1 - core), device_id_type=MESH)
-
-    def route(first_axis):
-        size_a, size_b = (rows_y, rows_x) if first_axis == "y" else (rows_x, rows_y)
-        here_a, here_b = (mine_y, mine_x) if first_axis == "y" else (mine_x, mine_y)
-
-        def index(z, a, b):
-            return z * plane + (a * rows_x + b if first_axis == "y" else b * rows_x + a)
-
-        sends = []
-        slot = 0
-        for step in range(1, depth):
-            sends.append((mine_z + step < depth, index(mine_z, here_a, here_b), index(mine_z + step, here_a, here_b), slot))
-            slot += 1
-
-        def start(items):
-            for _, shard, target, number in items:
-                for copy in copies(shard, target, number):
-                    copy.start()
-
-        for item in sends:
-            pl.when(item[0])(functools.partial(start, [item]))
-        for behind in range(depth):
-            z = mine_z - behind
-            items = []
-            shard = index(z, here_a, here_b)
-            for step in range(1, size_a):
-                items.append((z >= 0, shard, index(mine_z, (here_a + step) % size_a, here_b), slot))
-                slot += 1
-            for step in range(1, size_b):
-                items.append((z >= 0, shard, index(mine_z, here_a, (here_b + step) % size_b), slot))
-                slot += 1
-            sends += items
-
-            def forward(items=items, shard=shard, behind=behind):
-                if behind:
+        across(shard, core).start()
+
+    near_y = rows_y - 1
+    near_x = rows_x - 1
+    near = near_y + near_x
+
+    def both_ways(behind):
+        shard = place(behind, 0, 0)
+        for step in range(1, rows_x):
+            yield shard, place(0, 0, step), near_y + step - 1
+        for step in range(1, rows_y):
+            yield shard, place(0, step, 0), step - 1
+
+    def onward(behind, first_axis):
+        if first_axis == "y":
+            for step_a in range(1, rows_y):
+                for step_b in range(1, rows_x):
+                    yield place(behind, step_a, 0), place(0, 0, step_b), near + (step_a - 1) * near_x + step_b - 1
+        else:
+            for step_a in range(1, rows_x):
+                for step_b in range(1, rows_y):
+                    yield place(behind, 0, step_a), place(0, step_b, 0), near + (step_a - 1) * near_y + step_b - 1
+
+    def column(behind):
+        if not isinstance(behind, int):
+            arrived(place(behind, 0, 0))
+        for shard, target, slot in both_ways(behind):
+            start(shard, target, send_near.at[behind, slot])
+
+    def neighbours(behind):
+        def along(first_axis):
+            waited = []
+            for shard, target, slot in onward(behind, first_axis):
+                key = slot
+                inner = (rows_x if first_axis == "y" else rows_y) - 1
+                if (slot - near) % inner == 0:
                     arrived(shard)
-                start(items)
-                if behind:
-                    across(shard).start()
-
-            pl.when(z >= 0)(forward)
-        for behind in range(depth):
-            z = mine_z - behind
-            for step_a in range(1, size_a):
-                shard = index(z, (here_a + size_a - step_a) % size_a, here_b)
-                items = []
-                for step in range(1, size_b):
-                    items.append((z >= 0, shard, index(mine_z, here_a, (here_b + step) % size_b), slot))
-                    slot += 1
-                sends += items
-
-                def relay(items=items, shard=shard):
-                    arrived(shard)
-                    start(items)
-                    across(shard).start()
-
-                pl.when(z >= 0)(relay)
-        for behind in range(depth):
-            z = mine_z - behind
-            for step_b in range(1, size_b):
-                for step_a in range(size_a):
-                    shard = index(z, (here_a + size_a - step_a) % size_a, (here_b + size_b - step_b) % size_b)
-
-                    def last(shard=shard):
-                        arrived(shard)
-                        across(shard).start()
-
-                    pl.when(z >= 0)(last)
-        for behind in range(depth):
-            z = mine_z - behind
-
-            def settle(z=z):
-                for place in range(plane):
-
-                    def finish_half(shard=z * plane + place):
-                        other_half(shard).wait_recv()
-                        across(shard).wait_send()
-
-                    pl.when(z * plane + place != me)(finish_half)
-
-            pl.when(z >= 0)(settle)
-        for item in sends:
-
-            def sent(item=item):
-                for copy in copies(item[1], item[2], item[3]):
-                    copy.wait_send()
-
-            pl.when(item[0])(sent)
-
-    pl.when(core == 0)(functools.partial(route, "y"))
-    pl.when(core == 1)(functools.partial(route, "x"))
-
-
-def gather_keys(dims, kv, cum):
+                start(shard, target, send_near.at[behind, slot])
+            if first_axis == "y":
+                if near_x == 0:
+                    for step in range(1, rows_y):
+                        arrived(place(behind, step, 0))
+                for step in range(1, rows_x):
+                    arrived(place(behind, 0, step))
+            else:
+                if near_y == 0:
+                    for step in range(1, rows_x):
+                        arrived(place(behind, 0, step))
+                for step in range(1, rows_y):
+                    arrived(place(behind, step, 0))
+
+        pl.when(core == 0)(functools.partial(along, "y"))
+        pl.when(core == 1)(functools.partial(along, "x"))
+
+    def corners(behind):
+        for off_y in range(1, rows_y):
+            for off_x in range(1, rows_x):
+                arrived(place(behind, off_y, off_x))
+
+    def far(step):
+        return copies(me, (mine_z + step) * plane + me % plane, send_far.at[step])
+
+    column(0)
+    for step in range(1, depth):
+
+        def send_up(step=step):
+            for copy in far(step):
+                copy.start()
+
+        pl.when(mine_z + step < depth)(send_up)
+
+    def attend(shard, own):
+        gates = cums[shard]
+        picked = bf16_pieces(gates[:heads_small] * (-math.sqrt(size_small)))
+        if extra_s > 3 * heads_small:
+            picked.append(jnp.zeros((extra_s - 3 * heads_small, tokens), jnp.float32))
+        table[shard, :extra_s, :] = jnp.concatenate(picked, axis=0).astype(jnp.bfloat16)
+        picked = bf16_pieces(gates[heads_small:heads] * (-math.sqrt(size_large)))
+        if extra_l > 3 * heads_large:
+            picked.append(jnp.zeros((extra_l - 3 * heads_large, tokens), jnp.float32))
+        table[shard, gate_l:, :] = jnp.concatenate(picked, axis=0).astype(jnp.bfloat16)
+        for h in range(heads):
+            small = h < heads_small
+            size = size_small if small else size_large
+            scale = size ** (-0.5) * log2e
+            query = qs[h] if small else ql[h - heads_small]
+            keys = table[shard, :small_v, :] if small else table[shard, large_k:, :]
+            values = table[shard, small_v:large_v, :] if small else table[shard, large_v:large_k, :]
+            acc_ref, number = (acc_s, h) if small else (acc_l, h - heads_small)
+            scores = jnp.dot(query, keys, preferred_element_type=jnp.float32)
+            if own:
+                key_pos = lax.broadcasted_iota(jnp.int32, (tokens, tokens), 1)
+                query_pos = lax.broadcasted_iota(jnp.int32, (tokens, tokens), 0)
+                scores = jnp.where(key_pos <= query_pos, scores, far_score)
+            parts = [scores[:, j * 128:(j + 1) * 128] for j in range(tokens // 128)]
+            newest = jnp.max(functools.reduce(jnp.maximum, parts), axis=-1, keepdims=True)
+            if own:
+                newest = jnp.broadcast_to(newest, (tokens, 128))
+            else:
+                before = top[h]
+                newest = jnp.maximum(before, newest)
+                factor = jnp.exp2((before - newest) * scale)
+            scaled = newest * scale
+            found = [jnp.exp2(part * scale - scaled) for part in parts]
+            partial_sum = functools.reduce(jnp.add, found)
+            product = lax.dot_general(
+                jnp.concatenate(found, axis=1).astype(jnp.bfloat16), values,
+                (((1,), (1,)), ((), ())), preferred_element_type=jnp.float32)
+            top[h] = newest
+            if own:
+                total[h] = partial_sum
+                acc_ref[number] = product
+            else:
+                total[h] = total[h] * factor + partial_sum
+                acc_ref[number] = acc_ref[number] * factor[:, :size] + product
+
+    attend(me, True)
+    pl.when(mine_z >= 1)(lambda: column(jnp.int32(1)))
+    neighbours(0)
+    order = [(0, 0)] + [(step, 0) for step in range(1, rows_y)] + [(0, step) for step in range(1, rows_x)]
+    order += [(a, b) for a in range(1, rows_y) for b in range(1, rows_x)]
+
+    def step_of(number, _):
+        behind = number // plane
+        turn = number % plane
+        pl.when((turn == 0) & (behind + 1 <= mine_z))(lambda: column(behind + 1))
+        pl.when(turn == min(2, plane - 1))(lambda: corners(behind))
+        pl.when((turn == plane - 1) & (behind + 1 <= mine_z))(lambda: neighbours(behind + 1))
+        off_y = jnp.int32(0)
+        off_x = jnp.int32(0)
+        for index, (a, b) in enumerate(order):
+            off_y = jnp.where(turn == index, a, off_y)
+            off_x = jnp.where(turn == index, b, off_x)
+        shard = place(behind, off_y, off_x)
+        across(shard, 1 - core).wait_recv()
+        pl.when(shard < me)(lambda: attend(shard, False))
+        return 0
+
+    lax.fori_loop(1, (mine_z + 1) * plane, step_of, 0)
+
+    keep = tokens // 2
+    width_s = heads_small * size_small
+    width_l = heads_large * size_large
+    for mine in (False, True):
+        rows = pl.ds(pl.multiple_of((core if mine else 1 - core) * keep, keep), keep)
+        columns = []
+        for h in range(heads):
+            small = h < heads_small
+            sums = jnp.sum(total[h, rows, :], axis=-1, keepdims=True)
+            values = acc_s[h, rows, :] if small else acc_l[h - heads_small, rows, :]
+            columns.append((values / sums).astype(jnp.bfloat16))
+        joined_s = jnp.concatenate(columns[:heads_small], axis=1)
+        joined_l = jnp.concatenate(columns[heads_small:], axis=1)
+        if mine:
+            whole[:, pl.ds(pl.multiple_of(core * width_s, 128), width_s)] = joined_s
+            whole[:, pl.ds(pl.multiple_of(2 * width_s + core * width_l, 128), width_l)] = joined_l
+        else:
+            stage[:, :width_s] = joined_s
+            stage[:, width_s:] = joined_l
+
+    def swap(which):
+        return (
+            pltpu.make_async_remote_copy(
+                src_ref=stage.at[:, pl.ds(0, width_s)],
+                dst_ref=whole.at[:, pl.ds(pl.multiple_of(which * width_s, 128), width_s)],
+                send_sem=swap_send.at[0], recv_sem=swap_recv.at[0],
+                device_id=(me, 1 - core), device_id_type=MESH),
+            pltpu.make_async_remote_copy(
+                src_ref=stage.at[:, pl.ds(width_s, width_l)],
+                dst_ref=whole.at[:, pl.ds(pl.multiple_of(2 * width_s + which * width_l, 128), width_l)],
+                send_sem=swap_send.at[1], recv_sem=swap_recv.at[1],
+                device_id=(me, 1 - core), device_id_type=MESH),
+        )
+
+    for copy in swap(core):
+        copy.start()
+    for load in loads:
+        load.wait()
+    for step in range(1, depth):
+
+        def sent_up(step=step):
+            for copy in far(step):
+                copy.wait_send()
+
+        pl.when(mine_z + step < depth)(sent_up)
+
+    def sent(behind, _):
+        for shard, target, slot in both_ways(behind):
+            for copy in copies(shard, target, send_near.at[behind, slot]):
+                copy.wait_send()
+        for slot in range(near, near + near_y * near_x):
+            for copy in copies(me, me, send_near.at[behind, slot]):
+                copy.wait_send()
+
+        def crossed(number, _):
+            shard = (mine_z - behind) * plane + number
+            pl.when(shard != me)(lambda: across(shard, core).wait_send())
+            return 0
+
+        lax.fori_loop(0, plane, crossed, 0)
+        return 0
+
+    lax.fori_loop(0, mine_z + 1, sent, 0)
+    for copy in swap(1 - core):
+        copy.wait_recv()
+    columns = weights.shape[1]
+    tile = 512
+
+    def project(number, squares):
+        span = pl.ds(pl.multiple_of(number * tile, tile), tile)
+        part = jnp.dot(whole[...], weights[:, span], preferred_element_type=jnp.float32)
+        mixer[:, span] = part
+        square = part * part
+        return squares + functools.reduce(jnp.add, [square[:, j * 128:(j + 1) * 128] for j in range(tile // 128)])
+
+    squares = lax.fori_loop(0, columns // tile, project, jnp.zeros((keep, 128), jnp.float32))
+    mean = jnp.sum(squares, axis=-1, keepdims=True) * (1.0 / columns)
+    mixed = (
+        residual[...].astype(jnp.float32) + mixer[...] * lax.rsqrt(mean + norm_eps) * gain_mix[...]
+    ).astype(jnp.bfloat16)
+    mixed_ref[...] = mixed
+    routed_ref[...] = rms_scale(mixed.astype(jnp.float32), gain_route[...]).astype(jnp.bfloat16)
+    for copy in swap(core):
+        copy.wait_send()
+
+
+def mix(dims, queries_small, queries_large, kv_small, kv_large, cum_small, cum_large, residual, gain_mix, gain_route, out_small, out_large):
     shards = lax.axis_size("sp")
     depth, rows_y, rows_x = dims
-    slots = depth - 1 + depth * (rows_y + rows_x - 2) + depth * (rows_y - 1) * (rows_x - 1)
+    tokens = queries_small.shape[0]
+    heads_small = cum_small.shape[0]
+    heads_large = cum_large.shape[0]
+    size_small = kv_small.shape[1] // 2
+    size_large = kv_large.shape[1] // 2
+    heads = heads_small + heads_large
+    extra_s = round_up(3 * heads_small, 32)
+    extra_l = round_up(3 * heads_large, 16)
+    rows = extra_s + 2 * size_small + 2 * size_large + extra_l
+    near = rows_y + rows_x - 2 + (rows_y - 1) * (rows_x - 1)
+    keep, columns = residual.shape
     dma = pltpu.SemaphoreType.DMA
+    vmem = pl.BlockSpec(memory_space=pltpu.VMEM)
+    hbm = pl.BlockSpec(memory_space=pl.ANY)
+    bf16, f32 = jnp.bfloat16, jnp.float32
     return pl.pallas_call(
-        functools.partial(gather_kernel, dims),
+        functools.partial(mix_kernel, dims, (heads_small, heads_large, size_small, size_large)),
         out_shape=(
-            jax.ShapeDtypeStruct((shards,) + kv.shape, kv.dtype),
-            jax.ShapeDtypeStruct((shards,) + cum.shape, cum.dtype),
+            jax.ShapeDtypeStruct(residual.shape, bf16),
+            jax.ShapeDtypeStruct(residual.shape, bf16),
         ),
-        in_specs=[pl.BlockSpec(memory_space=pltpu.VMEM)] * 2,
-        out_specs=(pl.BlockSpec(memory_space=pltpu.VMEM),) * 2,
+        in_specs=[vmem] * 9 + [hbm] * 2,
+        out_specs=(vmem,) * 2,
         scratch_shapes=[
-            dma((slots,)), dma((slots,)), dma((shards,)), dma((shards,)), dma((shards,)), dma((shards,)), dma((2,)),
+            pltpu.VMEM((shards, rows, tokens), bf16),
+            pltpu.VMEM((shards, heads, tokens), f32),
+            pltpu.VMEM((heads_small, tokens, extra_s + size_small), bf16),
+            pltpu.VMEM((heads_large, tokens, size_large + extra_l), bf16),
+            pltpu.VMEM((heads, tokens, 128), f32),
+            pltpu.VMEM((heads, tokens, 128), f32),
+            pltpu.VMEM((heads_small, tokens, size_small), f32),
+            pltpu.VMEM((heads_large, tokens, size_large), f32),
+            pltpu.VMEM((keep, heads_small * size_small + heads_large * size_large), bf16),
+            pltpu.VMEM((keep, out_small.shape[0] + out_large.shape[0]), bf16),
+            pltpu.VMEM((out_small.shape[0] + out_large.shape[0], columns), bf16),
+            pltpu.VMEM((keep, columns), f32),
+            dma((depth, 2)), dma((depth, near, 2)), dma((shards,)), dma((shards,)), dma((shards,)), dma((shards,)),
+            dma((2,)), dma((2,)), dma((2,)),
         ],
-        compiler_params=pltpu.CompilerParams(collective_id=0, has_side_effects=True),
-        name="gather_keys",
-    )(kv, cum)
-
-
-def attend_kernel(head_shape, group, q_small, q_large, kv_all, cum_all, o_small, o_large, qs, ql, top, total, acc_s, acc_l):
-    heads_small, heads_large, size_small, size_large = head_shape
-    me = lax.axis_index("sp")
-    tokens = q_small.shape[0]
-    width = group * tokens
-    for h in range(heads_small):
-        qs[h] = q_small[:, h * size_small:(h + 1) * size_small]
-    for h in range(heads_large):
-        ql[h] = q_large[:, h * size_large:(h + 1) * size_large]
-    top[...] = jnp.full_like(top, far_score)
-    total[...] = jnp.zeros_like(total)
-    acc_s[...] = jnp.zeros_like(acc_s)
-    acc_l[...] = jnp.zeros_like(acc_l)
-
-    def block(number, masked):
-        first = number * group
-
-        def run(heads, base, q_ref, acc_ref, column, size):
-            scale = size ** (-0.5) * log2e
-
-            def one(h):
-                keys = kv_all[pl.ds(first, group), :, column:column + size].reshape(width, size)
-                values = kv_all[pl.ds(first, group), :, column + size:column + 2 * size].reshape(width, size)
-                gates = jnp.concatenate(
-                    [cum_all[first + j, pl.ds(base + h, 1), :] for j in range(group)], axis=1
-                ) * log2e
-                scores = lax.dot_general(
-                    q_ref[h], keys, (((1,), (1,)), ((), ())), preferred_element_type=jnp.float32
-                ) * scale - gates
-                if masked:
-                    key_pos = lax.broadcasted_iota(jnp.int32, (tokens, width), 1) + first * tokens
-                    query_pos = lax.broadcasted_iota(jnp.int32, (tokens, width), 0) + me * tokens
-                    scores = jnp.where(key_pos <= query_pos, scores, far_score)
-                before = top[base + h]
-                newest = jnp.maximum(before, jnp.max(scores, axis=-1, keepdims=True))
-                factor = jnp.exp2(before - newest)
-                weights = jnp.exp2(scores - newest[:, :1])
-                partial_sum = weights[:, :128]
-                for j in range(1, width // 128):
-                    partial_sum = partial_sum + weights[:, j * 128:(j + 1) * 128]
-                product = jnp.dot(
-                    weights.astype(jnp.bfloat16), values, preferred_element_type=jnp.float32
-                )
-                return (
-                    newest,
-                    total[base + h] * factor + partial_sum,
-                    acc_ref[h] * factor[:, :size] + product,
-                )
-
-            together = math.gcd(heads, 2)
-
-            def several(number, _):
-                found = [one(number * together + j) for j in range(together)]
-                for j in range(together):
-                    h = number * together + j
-                    top[base + h], total[base + h], acc_ref[h] = found[j]
-                return 0
-
-            lax.fori_loop(0, heads // together, several, 0)
-
-        run(heads_small, 0, qs, acc_s, 0, size_small)
-        run(heads_large, heads_small, ql, acc_l, 2 * size_small, size_large)
-
-    last = me // group
-
-    def whole(number, _):
-        block(number, False)
-        return 0
-
-    lax.fori_loop(0, last, whole, 0)
-    block(last, True)
-    for h in range(heads_small):
-        o_small[:, h * size_small:(h + 1) * size_small] = (
-            acc_s[h] / jnp.sum(total[h], axis=-1, keepdims=True)
-        ).astype(o_small.dtype)
-    for h in range(heads_large):
-        o_large[:, h * size_large:(h + 1) * size_large] = (
-            acc_l[h] / jnp.sum(total[heads_small + h], axis=-1, keepdims=True)
-        ).astype(o_large.dtype)
-
-
-def attend(queries_small, queries_large, kv_all, cum_all, head_shape, group):
-    heads_small, heads_large, size_small, size_large = head_shape
-    tokens = queries_small.shape[0]
-    heads = heads_small + heads_large
-    return pl.pallas_call(
-        functools.partial(attend_kernel, head_shape, group),
-        out_shape=(
-            jax.ShapeDtypeStruct(queries_small.shape, jnp.bfloat16),
-            jax.ShapeDtypeStruct(queries_large.shape, jnp.bfloat16),
-        ),
-        in_specs=[pl.BlockSpec(memory_space=pltpu.VMEM)] * 4,
-        out_specs=(pl.BlockSpec(memory_space=pltpu.VMEM),) * 2,
-        scratch_shapes=[
-            pltpu.VMEM((heads_small, tokens, size_small), jnp.bfloat16),
-            pltpu.VMEM((heads_large, tokens, size_large), jnp.bfloat16),
-            pltpu.VMEM((heads, tokens, 128), jnp.float32),
-            pltpu.VMEM((heads, tokens, 128), jnp.float32),
-            pltpu.VMEM((heads_small, tokens, size_small), jnp.float32),
-            pltpu.VMEM((heads_large, tokens, size_large), jnp.float32),
-        ],
-        compiler_params=pltpu.CompilerParams(vmem_limit_bytes=56 * 1024 * 1024),
-        name="attend",
-    )(queries_small, queries_large, kv_all, cum_all)
+        compiler_params=pltpu.CompilerParams(
+            collective_id=0, has_side_effects=True, vmem_limit_bytes=56 * 1024 * 1024),
+        name="mix",
+    )(queries_small, queries_large, kv_small, kv_large, cum_small, cum_large, residual,
+      gain_mix.reshape(1, columns), gain_route.reshape(1, columns), out_small, out_large)
 
 
 def greet(depth, plane, cores, me, core):
@@ -564,35 +671,11 @@
     route,
     route_bias,
 ):
-    tokens_here = queries_small.shape[0]
-    heads_small = cum_small.shape[0]
-    heads_large = cum_large.shape[0]
-    size_small = kv_small.shape[1] // 2
-    size_large = kv_large.shape[1] // 2
-    kv_all, cum_all = gather_keys(
-        dims,
-        jnp.concatenate([kv_small, kv_large], axis=1),
-        jnp.concatenate([cum_small, cum_large], axis=0),
+    row_count = residual.shape[0]
+    mixed, routed = mix(
+        dims, queries_small, queries_large, kv_small, kv_large, cum_small, cum_large, residual,
+        gain_mix, gain_route, out_small, out_large,
     )
-    group = math.gcd(dims[1] * dims[2], 4)
-    attn_small, attn_large = attend(
-        queries_small,
-        queries_large,
-        kv_all,
-        cum_all,
-        (heads_small, heads_large, size_small, size_large),
-        group,
-    )
-    row_count = tokens_here // lax.axis_size("tp")
-    whole_small, whole_large = (
-        lax.all_to_all(attn_small, "tp", split_axis=0, concat_axis=1, tiled=True),
-        lax.all_to_all(attn_large, "tp", split_axis=0, concat_axis=1, tiled=True),
-    )
-    mixer_out = jnp.dot(whole_small, out_small, preferred_element_type=jnp.float32) + jnp.dot(
-        whole_large, out_large, preferred_element_type=jnp.float32
-    )
-    mixed = (residual.astype(jnp.float32) + rms_scale(mixer_out, gain_mix)).astype(jnp.bfloat16)
-    routed = rms_scale(mixed.astype(jnp.float32), gain_route).astype(jnp.bfloat16)
     experts = lax.axis_size(("sp", "tp"))
     cores = lax.axis_size("tp")
     depth = dims[0]

time: 180 us -> 139 us (0.77)
  Pallas kernels: 142 us -> 115 us
  starting transfers between devices: 7.05 us -> 0 us
  local copies, waits for them, and re-layouts: 5 us -> 1.4 us
  matrix products: 19.8 us -> 17 us
    pallas_call x2 -> x1, Pallas kernels: 43.3 us -> 28.8 us  [mix(): pl.pallas_call(functools.partial(mix_kernel, dims, (heads_small, heads_la...]
    pallas_call x1, Pallas kernels: 52.7 us -> 40 us  [dispatch(): pl.pallas_call(functools.partial(dispatch_kernel, depth, cores), out_shap...]
    all_to_all x2 -> x0, starting transfers between devices: 7.05 us -> none  [the longest x1 3.59 us: on_device(): lax.all_to_all(attn_small, 'tp', split_axis=0, concat_axis=1, tiled=True)]
    dot_general x2 -> x0, matrix products: 5.98 us -> none  [the longest x1 3.06 us: on_device(): jnp.dot(whole_large, out_large, preferred_element_type=jnp.float32)]
    all_to_all x2 -> x0, local copies, waits for them, and re-layouts: 3.57 us -> none  [the longest x1 1.79 us: on_device(): lax.all_to_all(attn_large, 'tp', split_axis=0, concat_axis=1, tiled=True)]
    concatenate x2 -> x0, other arithmetic: 2.95 us -> none  [the longest x1 1.61 us: on_device(): jnp.concatenate([kv_small, kv_large], axis=1)]
    dot_general x1, matrix products: 3.69 us -> 5.91 us  [on_device(): jnp.dot(expert_rows, w_gate[0], preferred_element_type=jnp.float32)]
  transfers between devices with their start and end apart: 2 -> 0, of which waited for: 0 -> 0; matrix products, arithmetic and copies ran while one was open for 3% -> 0% of each run, Pallas kernels for 0% -> 0%
where the time goes in v1:
time: 139 us
  Pallas kernels  115 us (83%)
  matrix products  17 us (12%)
  other arithmetic  5.82 us (4%)
  local copies, waits for them, and re-layouts  1.4 us (1%)
    pallas_call x1, Pallas kernels, give_back(): pl.pallas_call(functools.partial(return_kernel, depth, cores), out_shape=...  45.9 us
    pallas_call x1, Pallas kernels, dispatch(): pl.pallas_call(functools.partial(dispatch_kernel, depth, cores), out_shap...  40 us
    pallas_call x1, Pallas kernels, mix(): pl.pallas_call(functools.partial(mix_kernel, dims, (heads_small, heads_la...  28.8 us
    dot_general x1, matrix products, on_device(): jnp.dot(hidden, w_down[0], preferred_element_type=jnp.float32)  9.23 us
    dot_general x1, matrix products, on_device(): jnp.dot(expert_rows, w_gate[0], preferred_element_type=jnp.float32)  5.91 us

profile of v1, /device:TPU:9, one launch (start us, length us, event | category | flops | bytes accessed | tf_op | source)
XLA Modules:
  0.0 139.1 jit_solution(4015430572204341841)
XLA Ops:
  0.0 0.7 fusion.27
  0.7 0.7 and_select_fusion.1
  1.4 0.2 convert_reduce_fusion.1
  1.6 0.7 fusion.21
  2.2 0.9 convert_reduce_fusion
  3.2 0.7 add_convert_fusion.1
  3.9 0.7 divide_bitcast_fusion.1
  4.6 0.2 select_reduce_fusion
  4.8 0.1 reshape.91
  4.9 28.8 %mix.1 = (bf16[128,2048]{1,0:T(8,128)(2,1)}, bf16[128,2048]{1,0:T(8,128)(2,1)}) custom-call(bf16[256,512]{1,0:T(8,128)(2,1)} %q_small.1, bf16[256,512]{1,0:T(8,128)(2,1)} %q_large.1, bf16[256,128]{1,0:T(8,128)(2,1)} %kv_small.1, bf16[256,256]{1,0:T(8,128)(2,1)} %kv_large.1, f32[8,256]{1,0:T(8,128)} %cum_small.1, f32[4,256]{1,0:T(4,128)} %cum_large.1, ...), custom_call_target="tpu_custom_call" | custom-call | tf_op jit(solution)/shard_map/mix/pallas_call | solution.py:382
  33.8 1.5 %convolution_convert_fusion = bf16[256,2048]{1,0:T(8,128)(2,1)S(1)} fusion(bf16[128,2048]{1,0:T(8,128)(2,1)} %get-tuple-element.10, s32[128]{0:T(128)S(1)} %fusion.21), kind=kOutput, calls=%fused_computation.7 | convolution fusion | flops 134774784 | bytes 1573376 | tf_op jit(solution)/shard_map/dot_general | solution.py:696
  35.2 40.0 %dispatch_rows.1 = (bf16[32,16,2048]{2,1,0:T(8,128)(2,1)S(1)}, f32[4,8,128]{2,1,0:T(8,128)S(1)}) custom-call(bf16[4,64,2048]{2,1,0:T(8,128)(2,1)S(1)} %bitcast.55, f32[4,8,128]{2,1,0:T(8,128)S(1)} %pad.4.meta_ref), custom_call_target="tpu_custom_call" | custom-call | tf_op jit(solution)/shard_map/dispatch_rows/pallas_call | solution.py:529
  75.2 0.0 copy-start
  75.2 1.3 copy-done
  76.5 5.9 %fusion.4 = f32[512,1024]{1,0:T(8,128)} fusion(bf16[512,2048]{1,0:T(8,128)(2,1)S(1)} %bitcast.57, bf16[1,2048,1024]{2,1,0:T(8,128)(2,1)} %param.29), kind=kOutput, calls=%fused_computation.4 | convolution fusion | flops 2147483648 | bytes 8388608 | tf_op jit(solution)/shard_map/dot_general | solution.py:704
  82.4 9.2 %fusion.6 = bf16[512,2048]{1,0:T(8,128)(2,1)S(1)} fusion(bf16[1,1024,2048]{2,1,0:T(8,128)(2,1)} %param.31, f32[512,1024]{1,0:T(8,128)} %fusion.4, bf16[512,2048]{1,0:T(8,128)(2,1)} %bitcast.58, bf16[1,2048,1024]{2,1,0:T(8,128)(2,1)} %param.30), kind=kOutput, calls=%fused_computation.6 | convolution fusion | flops 4299161600 | bytes 14680064 | tf_op jit(solution)/shard_map/dot_general | solution.py:707
  91.7 0.0 copy-start.1
  91.7 0.0 copy-start.2
  91.7 45.9 %return_rows.1 = bf16[4,64,2048]{2,1,0:T(8,128)(2,1)S(1)} custom-call(bf16[32,16,2048]{2,1,0:T(8,128)(2,1)S(1)} %bitcast.56, f32[4,8,128]{2,1,0:T(8,128)S(1)} %get-tuple-element.12.metas), custom_call_target="tpu_custom_call" | custom-call | tf_op jit(solution)/shard_map/return_rows/pallas_call | solution.py:632
  137.6 0.4 multiply_reduce_fusion
  138.0 0.0 copy-done.1
  138.0 0.0 copy-done.2
  138.1 1.0 add_convert_fusion
  (5 shorter events, 0.1 us)
Async XLA Ops:
  75.2 1.3 copy-start
  91.7 46.4 %copy-start.1 = (bf16[128,2048]{1,0:T(8,128)(2,1)S(1)}, bf16[128,2048]{1,0:T(8,128)(2,1)}, u32[]{:S(2)}) copy-start(bf16[128,2048]{1,0:T(8,128)(2,1)} %get-tuple-element.9) | copy-start | bytes 1572868
  91.7 46.4 %copy-start.2 = (f32[2048]{0:T(1024)S(1)}, f32[2048]{0:T(1024)}, u32[]{:S(2)}) copy-start(f32[2048]{0:T(1024)} %param.28) | copy-start | bytes 24580

commit v2 on v1

--- a/solution.py
+++ b/solution.py
@@ -421,7 +421,7 @@
         other = (here + step) % lanes
         target = me // plane * plane + other // cores
         pl.semaphore_signal(barrier, inc=1, device_id=(target, other % cores), device_id_type=MESH)
-    pl.semaphore_wait(barrier, depth - 1 + lanes - 1)
+    return depth - 1 + lanes - 1
 
 
 def distances(depth):
@@ -431,224 +431,262 @@
     return found
 
 
-def dispatch_kernel(depth, cores, rows_ref, meta_ref, received, metas, in_rows, stage, send_rows, send_meta, recv_rows, recv_meta, send_block, recv_block, own_sem):
+def as_column(row, eye):
+    return jnp.sum(jnp.where(eye, row, 0.0), axis=1, keepdims=True)
+
+
+def expert_kernel(
+    depth, cores,
+    routed_ref, mixed_ref, route_ref, bias_ref, gain_ref, w_gate, w_up, w_down,
+    result_ref,
+    out_rows, in_rows, out_meta, metas, spread, received, outs, back, combined, final, hidden, gate_w, up_w, down_w,
+    send_rows, recv_rows, send_meta, recv_meta, send_block, recv_block, send_back, recv_back, send_home, recv_home, load_sem,
+):
     me = lax.axis_index("sp")
     core = lax.axis_index("tp")
-    _, lanes, capacity, columns = stage.shape
+    _, lanes, capacity, columns = spread.shape
+    slots = in_rows.shape[1]
+    width = metas.shape[2]
+    tokens = routed_ref.shape[0]
     plane = lanes // cores
-    slots = rows_ref.shape[1]
+    count = lanes * capacity
     mine = me // plane
     here = me % plane * cores + core
-    own_rows = pltpu.make_async_copy(rows_ref.at[mine], in_rows.at[mine], own_sem.at[0, 0])
-    own_meta = pltpu.make_async_copy(meta_ref.at[mine], metas.at[mine], own_sem.at[0, 1])
-    own_rows.start()
-    own_meta.start()
-    greet(depth, plane, cores, me, core)
-
-    def along(other):
+    loads = (
+        pltpu.make_async_copy(w_gate.at[0], gate_w, load_sem.at[0]),
+        pltpu.make_async_copy(w_up.at[0], up_w, load_sem.at[1]),
+        pltpu.make_async_copy(w_down.at[0], down_w, load_sem.at[2]),
+    )
+    for load in loads:
+        load.start()
+    greeted = greet(depth, plane, cores, me, core)
+
+    row_of = lax.broadcasted_iota(jnp.int32, (tokens, tokens), 0)
+    lane_of = lax.broadcasted_iota(jnp.int32, (tokens, tokens), 1)
+    eye = row_of == lane_of
+    before = row_of < lane_of
+    ids = route_ref[...].astype(jnp.float32)
+    first, second = ids[0:1], ids[1:2]
+    groups = jnp.floor((first + 0.5) * (1.0 / lanes))
+    groups_col = as_column(groups, eye)
+    first_col = as_column(first, eye)
+    second_col = as_column(second, eye)
+
+    def total_rows(mask):
+        return jnp.sum(jnp.where(mask, 1.0, 0.0), axis=0, keepdims=True)
+
+    ranks = total_rows((groups_col == groups) & before)
+    places_first = (first - groups * lanes) * capacity + total_rows((first_col == first) & before) + 1.0
+    places_second = (
+        (second - groups * lanes) * capacity
+        + total_rows(first_col == second) + total_rows((second_col == second) & before) + 1.0
+    )
+    bias = bias_ref[...]
+    facts = [as_column(fact, eye) for fact in (places_first, places_second, jax.nn.sigmoid(bias), jax.nn.sigmoid(-bias))]
+    ranks_col = as_column(ranks, eye)
+    slot_rows = lax.broadcasted_iota(jnp.int32, (slots, tokens), 0).astype(jnp.float32)
+    slot_lanes = lax.broadcasted_iota(jnp.int32, (tokens, width), 1).astype(jnp.float32)
+    for group in range(depth):
+        table = jnp.where((slot_rows == ranks) & (groups == group), 1.0, 0.0).astype(jnp.bfloat16)
+        out_rows[group] = jnp.dot(table, routed_ref[...], preferred_element_type=jnp.float32).astype(jnp.bfloat16)
+        chosen = (slot_lanes == ranks_col) & (groups_col == group)
+        rows = [jnp.sum(jnp.where(chosen, fact, 0.0), axis=0, keepdims=True) for fact in facts]
+        out_meta[group] = jnp.concatenate(rows + [jnp.zeros((4, width), jnp.float32)], axis=0)
+    in_rows[mine] = out_rows[mine]
+    metas[mine] = out_meta[mine]
+    pl.semaphore_wait(pltpu.get_barrier_semaphore(), greeted)
+
+    def along(other, slot):
         target = (other * plane + me % plane, core)
         return (
             pltpu.make_async_remote_copy(
-                src_ref=rows_ref.at[other], dst_ref=in_rows.at[mine], send_sem=send_rows.at[other],
-                recv_sem=recv_rows.at[mine], device_id=target, device_id_type=MESH),
+                src_ref=out_rows.at[other], dst_ref=in_rows.at[slot], send_sem=send_rows.at[other],
+                recv_sem=recv_rows.at[slot], device_id=target, device_id_type=MESH),
             pltpu.make_async_remote_copy(
-                src_ref=meta_ref.at[other], dst_ref=metas.at[mine], send_sem=send_meta.at[other],
-                recv_sem=recv_meta.at[mine], device_id=target, device_id_type=MESH),
+                src_ref=out_meta.at[other], dst_ref=metas.at[slot], send_sem=send_meta.at[other],
+                recv_sem=recv_meta.at[slot], device_id=target, device_id_type=MESH),
         )
 
-    def incoming(other):
-        target = (other * plane + me % plane, core)
-        return (
-            pltpu.make_async_remote_copy(
-                src_ref=rows_ref.at[other], dst_ref=in_rows.at[other], send_sem=send_rows.at[other],
-                recv_sem=recv_rows.at[other], device_id=target, device_id_type=MESH),
-            pltpu.make_async_remote_copy(
-                src_ref=meta_ref.at[other], dst_ref=metas.at[other], send_sem=send_meta.at[other],
-                recv_sem=recv_meta.at[other], device_id=target, device_id_type=MESH),
-        )
-
-    def block(source, other, slot_of):
+    def outward(source, other, slot):
         return pltpu.make_async_remote_copy(
-            src_ref=stage.at[source, other], dst_ref=received.at[source * lanes + slot_of],
-            send_sem=send_block.at[source, other], recv_sem=recv_block.at[source, slot_of],
+            src_ref=spread.at[source, other], dst_ref=received.at[source, slot],
+            send_sem=send_block.at[source, other], recv_sem=recv_block.at[source, slot],
             device_id=(mine * plane + other // cores, other % cores), device_id_type=MESH)
 
-    def keep(source):
-        return pltpu.make_async_copy(
-            stage.at[source, here], received.at[source * lanes + here], own_sem.at[1, source])
+    def inward(source, other, slot):
+        return pltpu.make_async_remote_copy(
+            src_ref=outs.at[source, other], dst_ref=back.at[source, slot],
+            send_sem=send_back.at[source, other], recv_sem=recv_back.at[source, slot],
+            device_id=(mine * plane + other // cores, other % cores), device_id_type=MESH)
+
+    def homeward(other, slot):
+        return pltpu.make_async_remote_copy(
+            src_ref=combined.at[other], dst_ref=final.at[slot], send_sem=send_home.at[other],
+            recv_sem=recv_home.at[slot], device_id=(other * plane + me % plane, core), device_id_type=MESH)
 
     steps = distances(depth)
     for step in steps[1:]:
         other = mine + step
 
         def launch(other=other):
-            for copy in along(other):
+            for copy in along(other, mine):
                 copy.start()
 
         pl.when((other >= 0) & (other < depth))(launch)
-    own_rows.wait()
-    own_meta.wait()
-    for step in steps:
-        other = mine + step
-
-        def expand(other=other, step=step):
-            if step:
-                for copy in incoming(other):
-                    copy.wait_recv()
-            wanted = lax.broadcasted_iota(jnp.int32, (lanes * capacity, slots), 0).astype(jnp.float32) + 1.0
-            first = metas[other, 0:1, :slots]
-            second = metas[other, 1:2, :slots]
-            table = jnp.where((wanted == first) | (wanted == second), 1.0, 0.0).astype(jnp.bfloat16)
-            spread = jnp.dot(table, in_rows[other], preferred_element_type=jnp.float32)
-            for lane in range(lanes):
-                stage[other, lane] = spread[lane * capacity:(lane + 1) * capacity].astype(jnp.bfloat16)
-            for move in range(1, lanes):
-                block(other, (here + move) % lanes, here).start()
-            keep(other).start()
-
-        pl.when((other >= 0) & (other < depth))(expand)
-    for source in range(depth):
-        keep(source).wait()
+
+    orders = [[z + step for step in steps if 0 <= z + step < depth] for z in range(depth)]
+
+    def source_of(turn):
+        found = jnp.int32(0)
+        for z in range(depth):
+            for index in range(depth):
+                found = jnp.where((mine == z) & (turn == index), orders[z][index], found)
+        return found
+
+    def flat(ref, source):
+        if capacity % 16:
+            return jnp.concatenate(
+                [ref[source, lane].astype(jnp.float32) for lane in range(lanes)], axis=0).astype(jnp.bfloat16)
+        return ref[source].reshape(count, columns)
+
+    def split(ref, source, values, span):
+        for lane in range(lanes):
+            ref[source, lane, :, span] = values[lane * capacity:(lane + 1) * capacity].astype(jnp.bfloat16)
+
+    def expand(source):
+        def landed():
+            for copy in along(source, source):
+                copy.wait_recv()
+
+        pl.when(source != mine)(landed)
+        wanted = lax.broadcasted_iota(jnp.int32, (count, slots), 0).astype(jnp.float32) + 1.0
+        table = jnp.where(
+            (wanted == metas[source, 0:1, :slots]) | (wanted == metas[source, 1:2, :slots]), 1.0, 0.0
+        ).astype(jnp.bfloat16)
+        split(spread, source, jnp.dot(table, in_rows[source], preferred_element_type=jnp.float32), slice(None))
+        received[source, here] = spread[source, here]
         for move in range(1, lanes):
-            block(source, (here + move) % lanes, (here + move) % lanes).wait_recv()
-            block(source, (here + move) % lanes, here).wait_send()
+            outward(source, (here + move) % lanes, here).start()
+
+    tile = 256
+
+    def compute(source):
+        for move in range(1, lanes):
+            outward(source, (here + move) % lanes, (here + move) % lanes).wait_recv()
+        rows = flat(received, source)
+
+        def enter(number, _):
+            span = pl.ds(pl.multiple_of(number * tile, tile), tile)
+            gate = jnp.dot(rows, gate_w[:, span], preferred_element_type=jnp.float32)
+            up = jnp.dot(rows, up_w[:, span], preferred_element_type=jnp.float32)
+            hidden[:, span] = (jax.nn.silu(gate) * up).astype(jnp.bfloat16)
+            return 0
+
+        lax.fori_loop(0, gate_w.shape[1] // tile, enter, 0)
+
+        def leave(number, _):
+            span = pl.ds(pl.multiple_of(number * 2 * tile, 2 * tile), 2 * tile)
+            split(outs, source, jnp.dot(hidden[...], down_w[:, span], preferred_element_type=jnp.float32), span)
+            return 0
+
+        lax.fori_loop(0, columns // (2 * tile), leave, 0)
+        back[source, here] = outs[source, here]
+        for move in range(1, lanes):
+            inward(source, (here + move) % lanes, here).start()
+
+    def combine(source):
+        for move in range(1, lanes):
+            inward(source, (here + move) % lanes, (here + move) % lanes).wait_recv()
+        wanted = lax.broadcasted_iota(jnp.int32, (count, width), 0).astype(jnp.float32) + 1.0
+        shares = jnp.where(wanted == metas[source, 0:1, :], metas[source, 2:3, :], 0.0)
+        shares = shares + jnp.where(wanted == metas[source, 1:2, :], metas[source, 3:4, :], 0.0)
+        shares = shares.T[:slots]
+        high = shares.astype(jnp.bfloat16)
+        low = (shares - high.astype(jnp.float32)).astype(jnp.bfloat16)
+        picked = flat(back, source)
+        mixed = jnp.dot(high, picked, preferred_element_type=jnp.float32) + jnp.dot(
+            low, picked, preferred_element_type=jnp.float32)
+
+        def away():
+            combined[source] = mixed.astype(jnp.bfloat16)
+            homeward(source, mine).start()
+
+        def stay():
+            final[source] = mixed.astype(jnp.bfloat16)
+
+        pl.when(source != mine)(away)
+        pl.when(source == mine)(stay)
+
+    def turn_of(turn, _):
+        pl.when(turn < depth)(lambda: expand(source_of(turn)))
+
+        @pl.when(turn == 1)
+        def _():
+            for load in loads:
+                load.wait()
+
+        pl.when((turn >= 1) & (turn <= depth))(lambda: compute(source_of(turn - 1)))
+        pl.when(turn >= 2)(lambda: combine(source_of(turn - 2)))
+        return 0
+
+    lax.fori_loop(0, depth + 2, turn_of, 0)
     for step in steps[1:]:
         other = mine + step
 
-        def sent(other=other):
-            for copy in along(other):
+        def settle(other=other):
+            homeward(other, other).wait_recv()
+            homeward(other, mine).wait_send()
+            for copy in along(other, mine):
                 copy.wait_send()
 
-        pl.when((other >= 0) & (other < depth))(sent)
-
-
-def dispatch(rows, meta, lanes, cores, capacity):
-    depth, slots, columns = rows.shape
+        pl.when((other >= 0) & (other < depth))(settle)
+    for source in range(depth):
+        for move in range(1, lanes):
+            outward(source, (here + move) % lanes, here).wait_send()
+            inward(source, (here + move) % lanes, here).wait_send()
+    slot_all = lax.broadcasted_iota(jnp.int32, (tokens, depth * slots), 1).astype(jnp.float32)
+    table = jnp.where(slot_all == groups_col * slots + ranks_col, 1.0, 0.0).astype(jnp.bfloat16)
+    blended = jnp.dot(table, final[...].reshape(depth * slots, columns), preferred_element_type=jnp.float32)
+    result_ref[...] = (
+        mixed_ref[...].astype(jnp.float32) + rms_scale(blended, gain_ref[...])
+    ).astype(jnp.bfloat16)
+
+
+def experts_of(dims, routed, mixed, route, bias, gain, w_gate, w_up, w_down):
+    depth = dims[0]
+    cores = lax.axis_size("tp")
+    lanes = lax.axis_size(("sp", "tp")) // depth
+    tokens, columns = routed.shape
+    capacity = 4 * tokens // (depth * lanes)
+    slots = capacity * lanes // 2
+    width = round_up(slots, 128)
+    inner = w_gate.shape[2]
     dma = pltpu.SemaphoreType.DMA
     vmem = pl.BlockSpec(memory_space=pltpu.VMEM)
+    hbm = pl.BlockSpec(memory_space=pl.ANY)
+    bf16, f32 = jnp.bfloat16, jnp.float32
+    rows = pltpu.VMEM((depth, slots, columns), bf16)
+    blocks = pltpu.VMEM((depth, lanes, capacity, columns), bf16)
+    meta = pltpu.VMEM((depth, 8, width), f32)
     return pl.pallas_call(
-        functools.partial(dispatch_kernel, depth, cores),
-        out_shape=(
-            jax.ShapeDtypeStruct((depth * lanes, capacity, columns), rows.dtype),
-            jax.ShapeDtypeStruct(meta.shape, meta.dtype),
-        ),
-        in_specs=[vmem] * 2,
-        out_specs=(vmem,) * 2,
+        functools.partial(expert_kernel, depth, cores),
+        out_shape=jax.ShapeDtypeStruct(mixed.shape, bf16),
+        in_specs=[vmem] * 5 + [hbm] * 3,
+        out_specs=vmem,
         scratch_shapes=[
-            pltpu.VMEM(rows.shape, rows.dtype),
-            pltpu.VMEM((depth, lanes, capacity, columns), rows.dtype),
+            rows, rows, meta, meta, blocks, blocks, blocks, blocks, rows, rows,
+            pltpu.VMEM((lanes * capacity, inner), bf16),
+            pltpu.VMEM((columns, inner), bf16),
+            pltpu.VMEM((columns, inner), bf16),
+            pltpu.VMEM((inner, columns), bf16),
             dma((depth,)), dma((depth,)), dma((depth,)), dma((depth,)),
-            dma((depth, lanes)), dma((depth, lanes)), dma((2, max(depth, 2))),
+            dma((depth, lanes)), dma((depth, lanes)), dma((depth, lanes)), dma((depth, lanes)),
+            dma((depth,)), dma((depth,)), dma((3,)),
         ],
         compiler_params=pltpu.CompilerParams(
-            collective_id=1, has_side_effects=True, vmem_limit_bytes=48 * 1024 * 1024),
-        name="dispatch_rows",
-    )(rows, meta)
-
-
-def return_kernel(depth, cores, outs, metas, final, back, stage, send_block, recv_block, send_rows, recv_rows, own_sem):
-    me = lax.axis_index("sp")
-    core = lax.axis_index("tp")
-    _, lanes, capacity, columns = back.shape
-    plane = lanes // cores
-    slots = final.shape[1]
-    mine = me // plane
-    here = me % plane * cores + core
-    greet(depth, plane, cores, me, core)
-
-    def block(source, other, slot_of):
-        return pltpu.make_async_remote_copy(
-            src_ref=outs.at[source * lanes + other], dst_ref=back.at[source, slot_of],
-            send_sem=send_block.at[source, other], recv_sem=recv_block.at[source, slot_of],
-            device_id=(mine * plane + other // cores, other % cores), device_id_type=MESH)
-
-    def keep(source):
-        return pltpu.make_async_copy(
-            outs.at[source * lanes + here], back.at[source, here], own_sem.at[source])
-
-    def along(other, slot_of):
-        return pltpu.make_async_remote_copy(
-            src_ref=stage.at[other], dst_ref=final.at[slot_of], send_sem=send_rows.at[other],
-            recv_sem=recv_rows.at[slot_of], device_id=(other * plane + me % plane, core), device_id_type=MESH)
-
-    steps = distances(depth)[::-1]
-    for step in steps:
-        other = mine + step
-
-        def launch(other=other):
-            for move in range(1, lanes):
-                block(other, (here + move) % lanes, here).start()
-            keep(other).start()
-
-        pl.when((other >= 0) & (other < depth))(launch)
-    for step in steps:
-        other = mine + step
-
-        def combine(other=other, step=step):
-            keep(other).wait()
-            for move in range(1, lanes):
-                block(other, (here + move) % lanes, (here + move) % lanes).wait_recv()
-            count = lanes * capacity
-            width = metas.shape[2]
-            wanted = lax.broadcasted_iota(jnp.int32, (count, width), 0).astype(jnp.float32) + 1.0
-            weights = jnp.where(wanted == metas[other, 0:1, :], metas[other, 2:3, :], 0.0)
-            weights = weights + jnp.where(wanted == metas[other, 1:2, :], metas[other, 3:4, :], 0.0)
-            weights = weights.T[:slots]
-            high = weights.astype(jnp.bfloat16)
-            low = (weights - high.astype(jnp.float32)).astype(jnp.bfloat16)
-            if capacity % 16:
-                picked = jnp.concatenate(
-                    [back[other, lane].astype(jnp.float32) for lane in range(lanes)], axis=0
-                ).astype(jnp.bfloat16)
-            else:
-                picked = back[other].reshape(count, columns)
-            mixed = jnp.dot(high, picked, preferred_element_type=jnp.float32) + jnp.dot(
-                low, picked, preferred_element_type=jnp.float32)
-            if step:
-                stage[other] = mixed.astype(stage.dtype)
-                along(other, mine).start()
-            else:
-                final[other] = mixed.astype(final.dtype)
-
-        pl.when((other >= 0) & (other < depth))(combine)
-    for step in steps:
-        other = mine + step
-
-        def settle(other=other, step=step):
-            for move in range(1, lanes):
-                block(other, (here + move) % lanes, here).wait_send()
-            if step:
-                along(other, other).wait_recv()
-                along(other, mine).wait_send()
-
-        pl.when((other >= 0) & (other < depth))(settle)
-
-
-def give_back(outs, metas, lanes, cores, slots):
-    depth = metas.shape[0]
-    _, capacity, columns = outs.shape
-    dma = pltpu.SemaphoreType.DMA
-    vmem = pl.BlockSpec(memory_space=pltpu.VMEM)
-    return pl.pallas_call(
-        functools.partial(return_kernel, depth, cores),
-        out_shape=jax.ShapeDtypeStruct((depth, slots, columns), outs.dtype),
-        in_specs=[vmem] * 2,
-        out_specs=vmem,
-        scratch_shapes=[
-            pltpu.VMEM((depth, lanes, capacity, columns), outs.dtype),
-            pltpu.VMEM((depth, slots, columns), outs.dtype),
-            dma((depth, lanes)), dma((depth, lanes)), dma((depth,)), dma((depth,)), dma((depth,)),
-        ],
-        compiler_params=pltpu.CompilerParams(
-            collective_id=2, has_side_effects=True, vmem_limit_bytes=48 * 1024 * 1024),
-        name="return_rows",
-    )(outs, metas)
-
-
-def earlier_same(ids):
-    order = jnp.arange(ids.shape[0], dtype=jnp.int32)
-    same = (ids[:, None] == ids[None, :]) & (order[None, :] < order[:, None])
-    return jnp.sum(same.astype(jnp.int32), axis=1)
+            collective_id=1, has_side_effects=True, vmem_limit_bytes=60 * 1024 * 1024),
+        name="experts",
+    )(routed, mixed, route, bias.reshape(1, tokens), gain.reshape(1, columns), w_gate, w_up, w_down)
 
 
 def on_device(
@@ -671,48 +709,11 @@
     route,
     route_bias,
 ):
-    row_count = residual.shape[0]
     mixed, routed = mix(
         dims, queries_small, queries_large, kv_small, kv_large, cum_small, cum_large, residual,
         gain_mix, gain_route, out_small, out_large,
     )
-    experts = lax.axis_size(("sp", "tp"))
-    cores = lax.axis_size("tp")
-    depth = dims[0]
-    lanes = experts // depth
-    capacity = 4 * row_count // experts
-    slots = capacity * lanes // 2
-    group_ids = route[0] // lanes
-    row_slots = group_ids * slots + earlier_same(group_ids)
-    row_table = row_slots[None, :] == jnp.arange(depth * slots, dtype=jnp.int32)[:, None]
-    flat_ids = route.reshape(2 * row_count)
-    places = (flat_ids % lanes * capacity + earlier_same(flat_ids) + 1).astype(jnp.float32)
-    facts = jnp.stack(
-        [places[:row_count], places[row_count:], jax.nn.sigmoid(route_bias), jax.nn.sigmoid(-route_bias)]
-    )
-    meta = jnp.sum(jnp.where(row_table[None], facts[:, None, :], 0.0), axis=2)
-    meta = meta.reshape(4, depth, slots).transpose(1, 0, 2)
-    meta = jnp.pad(meta, ((0, 0), (0, 4), (0, -slots % 128)))
-    outgoing = jnp.dot(
-        row_table.astype(jnp.bfloat16), routed, preferred_element_type=jnp.float32
-    ).astype(jnp.bfloat16)
-    received, metas = dispatch(
-        outgoing.reshape(depth, slots, routed.shape[1]), meta, lanes, cores, capacity
-    )
-    row_total = received.shape[0] * received.shape[1]
-    expert_rows = received.reshape(row_total, received.shape[2])
-    gate_pre = jnp.dot(expert_rows, w_gate[0], preferred_element_type=jnp.float32)
-    up_pre = jnp.dot(expert_rows, w_up[0], preferred_element_type=jnp.float32)
-    hidden = (jax.nn.silu(gate_pre) * up_pre).astype(jnp.bfloat16)
-    expert_out = jnp.dot(hidden, w_down[0], preferred_element_type=jnp.float32).astype(jnp.bfloat16)
-    returned = give_back(expert_out.reshape(received.shape), metas, lanes, cores, slots)
-    blended = lax.dot_general(
-        row_table.astype(jnp.bfloat16),
-        returned.reshape(depth * slots, routed.shape[1]),
-        (((0,), (0,)), ((), ())),
-        preferred_element_type=jnp.float32,
-    )
-    return (mixed.astype(jnp.float32) + rms_scale(blended, gain_blend)).astype(jnp.bfloat16)
+    return experts_of(dims, routed, mixed, route, route_bias, gain_blend, w_gate, w_up, w_down)
 
 
 def solution(mesh):

time: 139 us -> 118 us (0.85)
  the two profiles are of different devices: /device:TPU:9 before, /device:TPU:0 now
where the time goes in v2:
time: 118 us
  Pallas kernels  116 us (98%)
  local copies, waits for them, and re-layouts  1.88 us (2%)
    pallas_call x1, Pallas kernels, experts_of(): pl.pallas_call(functools.partial(expert_kernel, depth, cores), out_shape=...  94.2 us
    pallas_call x1, Pallas kernels, mix(): pl.pallas_call(functools.partial(mix_kernel, dims, (heads_small, heads_la...  22.2 us

profile of v2, /device:TPU:0, one launch (start us, length us, event | category | flops | bytes accessed | tf_op | source)
XLA Modules:
  0.0 118.3 jit_solution(459954409373131668)
XLA Ops:
  0.0 22.2 %mix.1 = (bf16[128,2048]{1,0:T(8,128)(2,1)}, bf16[128,2048]{1,0:T(8,128)(2,1)}) custom-call(bf16[256,512]{1,0:T(8,128)(2,1)} %q_small.1, bf16[256,512]{1,0:T(8,128)(2,1)} %q_large.1, bf16[256,128]{1,0:T(8,128)(2,1)} %kv_small.1, bf16[256,256]{1,0:T(8,128)(2,1)} %kv_large.1, f32[8,256]{1,0:T(8,128)} %cum_small.1, f32[4,256]{1,0:T(4,128)} %cum_large.1, ...), custom_call_target="tpu_custom_call" | custom-call | tf_op jit(solution)/shard_map/mix/pallas_call | solution.py:382
  22.2 94.2 %experts.1 = bf16[128,2048]{1,0:T(8,128)(2,1)} custom-call(bf16[128,2048]{1,0:T(8,128)(2,1)} %get-tuple-element.7.routed_ref, bf16[128,2048]{1,0:T(8,128)(2,1)} %get-tuple-element.8.mixed_ref, s32[2,128]{1,0:T(2,128)} %route_ref.1, f32[1,128]{1,0:T(1,128)} %bitcast.7, f32[1,2048]{1,0:T(1,128)} %bitcast.6, bf16[1,2048,1024]{2,1,0:T(8,128)(2,1)} %w_gate.1, ...), custom_call_target="tpu_custom_call" | custom-call | tf_op jit(solution)/shard_map/experts/pallas_call | solution.py:671
  116.4 1.9 %copy.19 = bf16[128,2048]{1,0:T(8,128)(2,1)} copy(bf16[128,2048]{1,0:T(8,128)(2,1)} %experts.1) | data formatting | bytes 1048576

commit v3 on v2

--- a/solution.py
+++ b/solution.py
@@ -37,12 +37,61 @@
     return -(-value // unit) * unit
 
 
-def mix_kernel(
+def greet(depth, plane, cores, me, core):
+    barrier = pltpu.get_barrier_semaphore()
+    lanes = plane * cores
+    here = me % plane * cores + core
+    for step in range(1, depth):
+        target = (me // plane + step) % depth * plane + me % plane
+        pl.semaphore_signal(barrier, inc=1, device_id=(target, core), device_id_type=MESH)
+    for step in range(1, lanes):
+        other = (here + step) % lanes
+        target = me // plane * plane + other // cores
+        pl.semaphore_signal(barrier, inc=1, device_id=(target, other % cores), device_id_type=MESH)
+    return depth - 1 + lanes - 1
+
+
+def distances(depth):
+    found = [0]
+    for step in range(1, depth):
+        found += [step, -step]
+    return found
+
+
+def as_column(row, eye):
+    return jnp.sum(jnp.where(eye, row, 0.0), axis=1, keepdims=True)
+
+
+def plan_of(depth):
+    if depth == 4:
+        texts = (
+            "E0 E1 F0 F1 E3 E2 F3 F2 C3 C2 C1 C0",
+            "E1 E0 E2 F1 F2 C2 C1 E3 F3 F0 C3 C0",
+            "E0 E2 E1 E3 F0 F2 F1 C0 F3 C1 C3 C2",
+            "E3 E1 E0 E2 F1 F3 C3 C1 F0 F2 C0 C2",
+        )
+        return [[("EFC".index(word[0]), int(word[1])) for word in text.split()] for text in texts]
+    plans = []
+    for z in range(depth):
+        order = [z + step for step in distances(depth) if 0 <= z + step < depth]
+        plan = []
+        for turn in range(depth + 2):
+            plan += [(0, order[turn])] if turn < depth else []
+            plan += [(1, order[turn - 1])] if 1 <= turn <= depth else []
+            plan += [(2, order[turn - 2])] if turn >= 2 else []
+        plans.append(plan)
+    return plans
+
+
+def layer_kernel(
     dims, head_shape,
-    q_small, q_large, kv_small, kv_large, cum_small, cum_large, residual, gain_mix, gain_route, out_small, out_large,
-    mixed_ref, routed_ref,
-    table, cums, qs, ql, top, total, acc_s, acc_l, stage, whole, weights, mixer,
+    q_small, q_large, kv_small, kv_large, cum_small, cum_large, residual, gain_mix, gain_route, route_ref, bias_ref, gain_ref,
+    out_small, out_large, w_gate, w_up, w_down,
+    result_ref,
+    table, cums, qs, ql, top, total, acc_s, acc_l, stage, whole, weights, mixer, mixed_ref, routing,
+    out_rows, in_rows, out_meta, metas, spread, received, outs, back, combined, final, hidden, gate_w, up_w, down_w,
     send_far, send_near, send_core, recv_kv, recv_cum, recv_core, swap_send, swap_recv, load_sem,
+    send_rows, recv_rows, send_meta, recv_meta, send_block, recv_block, send_back, recv_back, send_home, recv_home,
 ):
     heads_small, heads_large, size_small, size_large = head_shape
     depth, rows_y, rows_x = dims
@@ -53,6 +102,13 @@
     mine_y = me % plane // rows_x
     mine_x = me % rows_x
     tokens = q_small.shape[0]
+    _, lanes, capacity, columns = spread.shape
+    cores = lanes // (dims[1] * dims[2])
+    slots = in_rows.shape[1]
+    width = metas.shape[2]
+    keep = residual.shape[0]
+    count = lanes * capacity
+    here = me % plane * cores + core
     heads = heads_small + heads_large
     extra_s = round_up(3 * heads_small, 32)
     extra_l = round_up(3 * heads_large, 16)
@@ -68,20 +124,14 @@
         pltpu.make_async_copy(
             out_large, weights.at[pl.ds(out_small.shape[0], out_large.shape[0])], load_sem.at[1]),
     )
-    for load in loads:
+    expert_loads = (
+        pltpu.make_async_copy(w_gate.at[0], gate_w, load_sem.at[2]),
+        pltpu.make_async_copy(w_up.at[0], up_w, load_sem.at[3]),
+        pltpu.make_async_copy(w_down.at[0], down_w, load_sem.at[4]),
+    )
+    for load in loads + expert_loads:
         load.start()
-    barrier = pltpu.get_barrier_semaphore()
-    for step in range(1, depth):
-        target = (mine_z + step) % depth * plane + me % plane
-        pl.semaphore_signal(barrier, inc=1, device_id=(target, core), device_id_type=MESH)
-    for step in range(1, rows_y):
-        target = mine_z * plane + (mine_y + step) % rows_y * rows_x + mine_x
-        pl.semaphore_signal(barrier, inc=1, device_id=(target, core), device_id_type=MESH)
-    for step in range(1, rows_x):
-        target = mine_z * plane + mine_y * rows_x + (mine_x + step) % rows_x
-        pl.semaphore_signal(barrier, inc=1, device_id=(target, core), device_id_type=MESH)
-    pl.semaphore_signal(barrier, inc=1, device_id=(me, 1 - core), device_id_type=MESH)
-
+    greeted = greet(depth, plane, cores, me, core)
     def turned(block):
         width = block.shape[1]
         eye = jnp.where(
@@ -106,7 +156,37 @@
         picks = jnp.where((lanes_l % heads_large == h) & (lanes_l < 3 * heads_large), 1.0, 0.0)
         ql[h] = jnp.concatenate(
             [q_large[:, h * size_large:(h + 1) * size_large], picks.astype(jnp.bfloat16)], axis=1)
-    pl.semaphore_wait(barrier, depth - 1 + rows_y - 1 + rows_x - 1 + 1)
+    row_of = lax.broadcasted_iota(jnp.int32, (keep, keep), 0)
+    lane_of = lax.broadcasted_iota(jnp.int32, (keep, keep), 1)
+    eye = row_of == lane_of
+    before = row_of < lane_of
+    ids = route_ref[...].astype(jnp.float32)
+    first, second = ids[0:1], ids[1:2]
+    groups = jnp.floor((first + 0.5) * (1.0 / lanes))
+    groups_col = as_column(groups, eye)
+    first_col = as_column(first, eye)
+    second_col = as_column(second, eye)
+
+    def total_rows(mask):
+        return jnp.sum(jnp.where(mask, 1.0, 0.0), axis=0, keepdims=True)
+
+    ranks = total_rows((groups_col == groups) & before)
+    places_first = (first - groups * lanes) * capacity + total_rows((first_col == first) & before) + 1.0
+    places_second = (
+        (second - groups * lanes) * capacity
+        + total_rows(first_col == second) + total_rows((second_col == second) & before) + 1.0
+    )
+    bias = bias_ref[...]
+    facts = [as_column(fact, eye) for fact in (places_first, places_second, jax.nn.sigmoid(bias), jax.nn.sigmoid(-bias))]
+    ranks_col = as_column(ranks, eye)
+    slot_lanes = lax.broadcasted_iota(jnp.int32, (keep, width), 1).astype(jnp.float32)
+    for group in range(depth):
+        chosen = (slot_lanes == ranks_col) & (groups_col == group)
+        rows = [jnp.sum(jnp.where(chosen, fact, 0.0), axis=0, keepdims=True) for fact in facts]
+        out_meta[group] = jnp.concatenate(rows + [jnp.zeros((4, width), jnp.float32)], axis=0)
+    routing[0:1] = groups
+    routing[1:2] = ranks
+    pl.semaphore_wait(pltpu.get_barrier_semaphore(), greeted)
 
     def place(behind, off_y, off_x):
         return (mine_z - behind) * plane + (mine_y + off_y) % rows_y * rows_x + (mine_x + off_x) % rows_x
@@ -166,9 +246,7 @@
 
     def neighbours(behind):
         def along(first_axis):
-            waited = []
             for shard, target, slot in onward(behind, first_axis):
-                key = slot
                 inner = (rows_x if first_axis == "y" else rows_y) - 1
                 if (slot - near) % inner == 0:
                     arrived(shard)
@@ -198,7 +276,7 @@
         return copies(me, (mine_z + step) * plane + me % plane, send_far.at[step])
 
     column(0)
-    for step in range(1, depth):
+    for step in reversed(range(1, depth)):
 
         def send_up(step=step):
             for copy in far(step):
@@ -275,19 +353,18 @@
 
     lax.fori_loop(1, (mine_z + 1) * plane, step_of, 0)
 
-    keep = tokens // 2
     width_s = heads_small * size_small
     width_l = heads_large * size_large
     for mine in (False, True):
         rows = pl.ds(pl.multiple_of((core if mine else 1 - core) * keep, keep), keep)
-        columns = []
+        shown = []
         for h in range(heads):
             small = h < heads_small
             sums = jnp.sum(total[h, rows, :], axis=-1, keepdims=True)
             values = acc_s[h, rows, :] if small else acc_l[h - heads_small, rows, :]
-            columns.append((values / sums).astype(jnp.bfloat16))
-        joined_s = jnp.concatenate(columns[:heads_small], axis=1)
-        joined_l = jnp.concatenate(columns[heads_small:], axis=1)
+            shown.append((values / sums).astype(jnp.bfloat16))
+        joined_s = jnp.concatenate(shown[:heads_small], axis=1)
+        joined_l = jnp.concatenate(shown[heads_small:], axis=1)
         if mine:
             whole[:, pl.ds(pl.multiple_of(core * width_s, 128), width_s)] = joined_s
             whole[:, pl.ds(pl.multiple_of(2 * width_s + core * width_l, 128), width_l)] = joined_l
@@ -313,188 +390,33 @@
         copy.start()
     for load in loads:
         load.wait()
-    for step in range(1, depth):
-
-        def sent_up(step=step):
-            for copy in far(step):
-                copy.wait_send()
-
-        pl.when(mine_z + step < depth)(sent_up)
-
-    def sent(behind, _):
-        for shard, target, slot in both_ways(behind):
-            for copy in copies(shard, target, send_near.at[behind, slot]):
-                copy.wait_send()
-        for slot in range(near, near + near_y * near_x):
-            for copy in copies(me, me, send_near.at[behind, slot]):
-                copy.wait_send()
-
-        def crossed(number, _):
-            shard = (mine_z - behind) * plane + number
-            pl.when(shard != me)(lambda: across(shard, core).wait_send())
-            return 0
-
-        lax.fori_loop(0, plane, crossed, 0)
-        return 0
-
-    lax.fori_loop(0, mine_z + 1, sent, 0)
     for copy in swap(1 - core):
         copy.wait_recv()
-    columns = weights.shape[1]
-    tile = 512
+    span_w = 512
 
     def project(number, squares):
-        span = pl.ds(pl.multiple_of(number * tile, tile), tile)
+        span = pl.ds(pl.multiple_of(number * span_w, span_w), span_w)
         part = jnp.dot(whole[...], weights[:, span], preferred_element_type=jnp.float32)
         mixer[:, span] = part
         square = part * part
-        return squares + functools.reduce(jnp.add, [square[:, j * 128:(j + 1) * 128] for j in range(tile // 128)])
-
-    squares = lax.fori_loop(0, columns // tile, project, jnp.zeros((keep, 128), jnp.float32))
+        return squares + functools.reduce(jnp.add, [square[:, j * 128:(j + 1) * 128] for j in range(span_w // 128)])
+
+    squares = lax.fori_loop(0, columns // span_w, project, jnp.zeros((keep, 128), jnp.float32))
     mean = jnp.sum(squares, axis=-1, keepdims=True) * (1.0 / columns)
     mixed = (
         residual[...].astype(jnp.float32) + mixer[...] * lax.rsqrt(mean + norm_eps) * gain_mix[...]
     ).astype(jnp.bfloat16)
     mixed_ref[...] = mixed
-    routed_ref[...] = rms_scale(mixed.astype(jnp.float32), gain_route[...]).astype(jnp.bfloat16)
-    for copy in swap(core):
-        copy.wait_send()
-
-
-def mix(dims, queries_small, queries_large, kv_small, kv_large, cum_small, cum_large, residual, gain_mix, gain_route, out_small, out_large):
-    shards = lax.axis_size("sp")
-    depth, rows_y, rows_x = dims
-    tokens = queries_small.shape[0]
-    heads_small = cum_small.shape[0]
-    heads_large = cum_large.shape[0]
-    size_small = kv_small.shape[1] // 2
-    size_large = kv_large.shape[1] // 2
-    heads = heads_small + heads_large
-    extra_s = round_up(3 * heads_small, 32)
-    extra_l = round_up(3 * heads_large, 16)
-    rows = extra_s + 2 * size_small + 2 * size_large + extra_l
-    near = rows_y + rows_x - 2 + (rows_y - 1) * (rows_x - 1)
-    keep, columns = residual.shape
-    dma = pltpu.SemaphoreType.DMA
-    vmem = pl.BlockSpec(memory_space=pltpu.VMEM)
-    hbm = pl.BlockSpec(memory_space=pl.ANY)
-    bf16, f32 = jnp.bfloat16, jnp.float32
-    return pl.pallas_call(
-        functools.partial(mix_kernel, dims, (heads_small, heads_large, size_small, size_large)),
-        out_shape=(
-            jax.ShapeDtypeStruct(residual.shape, bf16),
-            jax.ShapeDtypeStruct(residual.shape, bf16),
-        ),
-        in_specs=[vmem] * 9 + [hbm] * 2,
-        out_specs=(vmem,) * 2,
-        scratch_shapes=[
-            pltpu.VMEM((shards, rows, tokens), bf16),
-            pltpu.VMEM((shards, heads, tokens), f32),
-            pltpu.VMEM((heads_small, tokens, extra_s + size_small), bf16),
-            pltpu.VMEM((heads_large, tokens, size_large + extra_l), bf16),
-            pltpu.VMEM((heads, tokens, 128), f32),
-            pltpu.VMEM((heads, tokens, 128), f32),
-            pltpu.VMEM((heads_small, tokens, size_small), f32),
-            pltpu.VMEM((heads_large, tokens, size_large), f32),
-            pltpu.VMEM((keep, heads_small * size_small + heads_large * size_large), bf16),
-            pltpu.VMEM((keep, out_small.shape[0] + out_large.shape[0]), bf16),
-            pltpu.VMEM((out_small.shape[0] + out_large.shape[0], columns), bf16),
-            pltpu.VMEM((keep, columns), f32),
-            dma((depth, 2)), dma((depth, near, 2)), dma((shards,)), dma((shards,)), dma((shards,)), dma((shards,)),
-            dma((2,)), dma((2,)), dma((2,)),
-        ],
-        compiler_params=pltpu.CompilerParams(
-            collective_id=0, has_side_effects=True, vmem_limit_bytes=56 * 1024 * 1024),
-        name="mix",
-    )(queries_small, queries_large, kv_small, kv_large, cum_small, cum_large, residual,
-      gain_mix.reshape(1, columns), gain_route.reshape(1, columns), out_small, out_large)
-
-
-def greet(depth, plane, cores, me, core):
-    barrier = pltpu.get_barrier_semaphore()
-    lanes = plane * cores
-    here = me % plane * cores + core
-    for step in range(1, depth):
-        target = (me // plane + step) % depth * plane + me % plane
-        pl.semaphore_signal(barrier, inc=1, device_id=(target, core), device_id_type=MESH)
-    for step in range(1, lanes):
-        other = (here + step) % lanes
-        target = me // plane * plane + other // cores
-        pl.semaphore_signal(barrier, inc=1, device_id=(target, other % cores), device_id_type=MESH)
-    return depth - 1 + lanes - 1
-
-
-def distances(depth):
-    found = [0]
-    for step in range(1, depth):
-        found += [step, -step]
-    return found
-
-
-def as_column(row, eye):
-    return jnp.sum(jnp.where(eye, row, 0.0), axis=1, keepdims=True)
-
-
-def expert_kernel(
-    depth, cores,
-    routed_ref, mixed_ref, route_ref, bias_ref, gain_ref, w_gate, w_up, w_down,
-    result_ref,
-    out_rows, in_rows, out_meta, metas, spread, received, outs, back, combined, final, hidden, gate_w, up_w, down_w,
-    send_rows, recv_rows, send_meta, recv_meta, send_block, recv_block, send_back, recv_back, send_home, recv_home, load_sem,
-):
-    me = lax.axis_index("sp")
-    core = lax.axis_index("tp")
-    _, lanes, capacity, columns = spread.shape
-    slots = in_rows.shape[1]
-    width = metas.shape[2]
-    tokens = routed_ref.shape[0]
-    plane = lanes // cores
-    count = lanes * capacity
-    mine = me // plane
-    here = me % plane * cores + core
-    loads = (
-        pltpu.make_async_copy(w_gate.at[0], gate_w, load_sem.at[0]),
-        pltpu.make_async_copy(w_up.at[0], up_w, load_sem.at[1]),
-        pltpu.make_async_copy(w_down.at[0], down_w, load_sem.at[2]),
-    )
-    for load in loads:
-        load.start()
-    greeted = greet(depth, plane, cores, me, core)
-
-    row_of = lax.broadcasted_iota(jnp.int32, (tokens, tokens), 0)
-    lane_of = lax.broadcasted_iota(jnp.int32, (tokens, tokens), 1)
-    eye = row_of == lane_of
-    before = row_of < lane_of
-    ids = route_ref[...].astype(jnp.float32)
-    first, second = ids[0:1], ids[1:2]
-    groups = jnp.floor((first + 0.5) * (1.0 / lanes))
-    groups_col = as_column(groups, eye)
-    first_col = as_column(first, eye)
-    second_col = as_column(second, eye)
-
-    def total_rows(mask):
-        return jnp.sum(jnp.where(mask, 1.0, 0.0), axis=0, keepdims=True)
-
-    ranks = total_rows((groups_col == groups) & before)
-    places_first = (first - groups * lanes) * capacity + total_rows((first_col == first) & before) + 1.0
-    places_second = (
-        (second - groups * lanes) * capacity
-        + total_rows(first_col == second) + total_rows((second_col == second) & before) + 1.0
-    )
-    bias = bias_ref[...]
-    facts = [as_column(fact, eye) for fact in (places_first, places_second, jax.nn.sigmoid(bias), jax.nn.sigmoid(-bias))]
-    ranks_col = as_column(ranks, eye)
-    slot_rows = lax.broadcasted_iota(jnp.int32, (slots, tokens), 0).astype(jnp.float32)
-    slot_lanes = lax.broadcasted_iota(jnp.int32, (tokens, width), 1).astype(jnp.float32)
+    routed = rms_scale(mixed.astype(jnp.float32), gain_route[...])
+
+
+    routed = routed.astype(jnp.bfloat16)
+    slot_rows = lax.broadcasted_iota(jnp.int32, (slots, keep), 0).astype(jnp.float32)
     for group in range(depth):
-        table = jnp.where((slot_rows == ranks) & (groups == group), 1.0, 0.0).astype(jnp.bfloat16)
-        out_rows[group] = jnp.dot(table, routed_ref[...], preferred_element_type=jnp.float32).astype(jnp.bfloat16)
-        chosen = (slot_lanes == ranks_col) & (groups_col == group)
-        rows = [jnp.sum(jnp.where(chosen, fact, 0.0), axis=0, keepdims=True) for fact in facts]
-        out_meta[group] = jnp.concatenate(rows + [jnp.zeros((4, width), jnp.float32)], axis=0)
-    in_rows[mine] = out_rows[mine]
-    metas[mine] = out_meta[mine]
-    pl.semaphore_wait(pltpu.get_barrier_semaphore(), greeted)
+        table_of = jnp.where((slot_rows == routing[1:2]) & (routing[0:1] == group), 1.0, 0.0).astype(jnp.bfloat16)
+        out_rows[group] = jnp.dot(table_of, routed, preferred_element_type=jnp.float32).astype(jnp.bfloat16)
+    in_rows[mine_z] = out_rows[mine_z]
+    metas[mine_z] = out_meta[mine_z]
 
     def along(other, slot):
         target = (other * plane + me % plane, core)
@@ -511,13 +433,13 @@
         return pltpu.make_async_remote_copy(
             src_ref=spread.at[source, other], dst_ref=received.at[source, slot],
             send_sem=send_block.at[source, other], recv_sem=recv_block.at[source, slot],
-            device_id=(mine * plane + other // cores, other % cores), device_id_type=MESH)
+            device_id=(mine_z * plane + other // cores, other % cores), device_id_type=MESH)
 
     def inward(source, other, slot):
         return pltpu.make_async_remote_copy(
             src_ref=outs.at[source, other], dst_ref=back.at[source, slot],
             send_sem=send_back.at[source, other], recv_sem=recv_back.at[source, slot],
-            device_id=(mine * plane + other // cores, other % cores), device_id_type=MESH)
+            device_id=(mine_z * plane + other // cores, other % cores), device_id_type=MESH)
 
     def homeward(other, slot):
         return pltpu.make_async_remote_copy(
@@ -526,22 +448,13 @@
 
     steps = distances(depth)
     for step in steps[1:]:
-        other = mine + step
+        other = mine_z + step
 
         def launch(other=other):
-            for copy in along(other, mine):
+            for copy in along(other, mine_z):
                 copy.start()
 
         pl.when((other >= 0) & (other < depth))(launch)
-
-    orders = [[z + step for step in steps if 0 <= z + step < depth] for z in range(depth)]
-
-    def source_of(turn):
-        found = jnp.int32(0)
-        for z in range(depth):
-            for index in range(depth):
-                found = jnp.where((mine == z) & (turn == index), orders[z][index], found)
-        return found
 
     def flat(ref, source):
         if capacity % 16:
@@ -558,12 +471,12 @@
             for copy in along(source, source):
                 copy.wait_recv()
 
-        pl.when(source != mine)(landed)
+        pl.when(source != mine_z)(landed)
         wanted = lax.broadcasted_iota(jnp.int32, (count, slots), 0).astype(jnp.float32) + 1.0
-        table = jnp.where(
+        spots = jnp.where(
             (wanted == metas[source, 0:1, :slots]) | (wanted == metas[source, 1:2, :slots]), 1.0, 0.0
         ).astype(jnp.bfloat16)
-        split(spread, source, jnp.dot(table, in_rows[source], preferred_element_type=jnp.float32), slice(None))
+        split(spread, source, jnp.dot(spots, in_rows[source], preferred_element_type=jnp.float32), slice(None))
         received[source, here] = spread[source, here]
         for move in range(1, lanes):
             outward(source, (here + move) % lanes, here).start()
@@ -609,34 +522,38 @@
 
         def away():
             combined[source] = mixed.astype(jnp.bfloat16)
-            homeward(source, mine).start()
+            homeward(source, mine_z).start()
 
         def stay():
             final[source] = mixed.astype(jnp.bfloat16)
 
-        pl.when(source != mine)(away)
-        pl.when(source == mine)(stay)
+        pl.when(source != mine_z)(away)
+        pl.when(source == mine_z)(stay)
+
+    plans = plan_of(depth)
 
     def turn_of(turn, _):
-        pl.when(turn < depth)(lambda: expand(source_of(turn)))
-
-        @pl.when(turn == 1)
-        def _():
-            for load in loads:
-                load.wait()
-
-        pl.when((turn >= 1) & (turn <= depth))(lambda: compute(source_of(turn - 1)))
-        pl.when(turn >= 2)(lambda: combine(source_of(turn - 2)))
+        found = jnp.int32(0)
+        for z in range(depth):
+            for index, (kind, source) in enumerate(plans[z]):
+                found = jnp.where((mine_z == z) & (turn == index), kind * depth + source, found)
+        kind = found // depth
+        source = found % depth
+        pl.when(kind == 0)(lambda: expand(source))
+        pl.when(kind == 1)(lambda: compute(source))
+        pl.when(kind == 2)(lambda: combine(source))
         return 0
 
-    lax.fori_loop(0, depth + 2, turn_of, 0)
+    for load in expert_loads:
+        load.wait()
+    lax.fori_loop(0, 3 * depth, turn_of, 0)
     for step in steps[1:]:
-        other = mine + step
+        other = mine_z + step
 
         def settle(other=other):
             homeward(other, other).wait_recv()
-            homeward(other, mine).wait_send()
-            for copy in along(other, mine):
+            homeward(other, mine_z).wait_send()
+            for copy in along(other, mine_z):
                 copy.wait_send()
 
         pl.when((other >= 0) & (other < depth))(settle)
@@ -644,23 +561,62 @@
         for move in range(1, lanes):
             outward(source, (here + move) % lanes, here).wait_send()
             inward(source, (here + move) % lanes, here).wait_send()
-    slot_all = lax.broadcasted_iota(jnp.int32, (tokens, depth * slots), 1).astype(jnp.float32)
-    table = jnp.where(slot_all == groups_col * slots + ranks_col, 1.0, 0.0).astype(jnp.bfloat16)
-    blended = jnp.dot(table, final[...].reshape(depth * slots, columns), preferred_element_type=jnp.float32)
+    for step in range(1, depth):
+
+        def sent_up(step=step):
+            for copy in far(step):
+                copy.wait_send()
+
+        pl.when(mine_z + step < depth)(sent_up)
+
+    def sent(behind, _):
+        for shard, target, slot in both_ways(behind):
+            for copy in copies(shard, target, send_near.at[behind, slot]):
+                copy.wait_send()
+        for slot in range(near, near + near_y * near_x):
+            for copy in copies(me, me, send_near.at[behind, slot]):
+                copy.wait_send()
+
+        def crossed(number, _):
+            shard = (mine_z - behind) * plane + number
+            pl.when(shard != me)(lambda: across(shard, core).wait_send())
+            return 0
+
+        lax.fori_loop(0, plane, crossed, 0)
+        return 0
+
+    lax.fori_loop(0, mine_z + 1, sent, 0)
+    for copy in swap(core):
+        copy.wait_send()
+    eye = lax.broadcasted_iota(jnp.int32, (keep, keep), 0) == lax.broadcasted_iota(jnp.int32, (keep, keep), 1)
+    slot_all = lax.broadcasted_iota(jnp.int32, (keep, depth * slots), 1).astype(jnp.float32)
+    places = jnp.where(slot_all == as_column(routing[0:1] * slots + routing[1:2], eye), 1.0, 0.0).astype(jnp.bfloat16)
+    blended = jnp.dot(places, final[...].reshape(depth * slots, columns), preferred_element_type=jnp.float32)
     result_ref[...] = (
         mixed_ref[...].astype(jnp.float32) + rms_scale(blended, gain_ref[...])
     ).astype(jnp.bfloat16)
 
 
-def experts_of(dims, routed, mixed, route, bias, gain, w_gate, w_up, w_down):
-    depth = dims[0]
-    cores = lax.axis_size("tp")
+def layer(dims, queries_small, queries_large, kv_small, kv_large, cum_small, cum_large, residual, gain_mix, gain_route, route, bias, gain_blend, out_small, out_large, w_gate, w_up, w_down):
+    shards = lax.axis_size("sp")
+    depth, rows_y, rows_x = dims
+    tokens = queries_small.shape[0]
+    heads_small = cum_small.shape[0]
+    heads_large = cum_large.shape[0]
+    size_small = kv_small.shape[1] // 2
+    size_large = kv_large.shape[1] // 2
+    heads = heads_small + heads_large
+    extra_s = round_up(3 * heads_small, 32)
+    extra_l = round_up(3 * heads_large, 16)
+    table_rows = extra_s + 2 * size_small + 2 * size_large + extra_l
+    near = rows_y + rows_x - 2 + (rows_y - 1) * (rows_x - 1)
+    keep, columns = residual.shape
     lanes = lax.axis_size(("sp", "tp")) // depth
-    tokens, columns = routed.shape
-    capacity = 4 * tokens // (depth * lanes)
+    capacity = 4 * keep // (depth * lanes)
     slots = capacity * lanes // 2
     width = round_up(slots, 128)
     inner = w_gate.shape[2]
+    joined = out_small.shape[0] + out_large.shape[0]
     dma = pltpu.SemaphoreType.DMA
     vmem = pl.BlockSpec(memory_space=pltpu.VMEM)
     hbm = pl.BlockSpec(memory_space=pl.ANY)
@@ -669,24 +625,42 @@
     blocks = pltpu.VMEM((depth, lanes, capacity, columns), bf16)
     meta = pltpu.VMEM((depth, 8, width), f32)
     return pl.pallas_call(
-        functools.partial(expert_kernel, depth, cores),
-        out_shape=jax.ShapeDtypeStruct(mixed.shape, bf16),
-        in_specs=[vmem] * 5 + [hbm] * 3,
+        functools.partial(layer_kernel, dims, (heads_small, heads_large, size_small, size_large)),
+        out_shape=jax.ShapeDtypeStruct(residual.shape, bf16),
+        in_specs=[vmem] * 12 + [hbm] * 5,
         out_specs=vmem,
         scratch_shapes=[
+            pltpu.VMEM((shards, table_rows, tokens), bf16),
+            pltpu.VMEM((shards, heads, tokens), f32),
+            pltpu.VMEM((heads_small, tokens, extra_s + size_small), bf16),
+            pltpu.VMEM((heads_large, tokens, size_large + extra_l), bf16),
+            pltpu.VMEM((heads, tokens, 128), f32),
+            pltpu.VMEM((heads, tokens, 128), f32),
+            pltpu.VMEM((heads_small, tokens, size_small), f32),
+            pltpu.VMEM((heads_large, tokens, size_large), f32),
+            pltpu.VMEM((keep, heads_small * size_small + heads_large * size_large), bf16),
+            pltpu.VMEM((keep, joined), bf16),
+            pltpu.VMEM((joined, columns), bf16),
+            pltpu.VMEM((keep, columns), f32),
+            pltpu.VMEM((keep, columns), bf16),
+            pltpu.VMEM((8, keep), f32),
             rows, rows, meta, meta, blocks, blocks, blocks, blocks, rows, rows,
             pltpu.VMEM((lanes * capacity, inner), bf16),
             pltpu.VMEM((columns, inner), bf16),
             pltpu.VMEM((columns, inner), bf16),
             pltpu.VMEM((inner, columns), bf16),
+            dma((depth, 2)), dma((depth, near, 2)), dma((shards,)), dma((shards,)), dma((shards,)), dma((shards,)),
+            dma((2,)), dma((2,)), dma((5,)),
             dma((depth,)), dma((depth,)), dma((depth,)), dma((depth,)),
             dma((depth, lanes)), dma((depth, lanes)), dma((depth, lanes)), dma((depth, lanes)),
-            dma((depth,)), dma((depth,)), dma((3,)),
+            dma((depth,)), dma((depth,)),
         ],
         compiler_params=pltpu.CompilerParams(
-            collective_id=1, has_side_effects=True, vmem_limit_bytes=60 * 1024 * 1024),
-        name="experts",
-    )(routed, mixed, route, bias.reshape(1, tokens), gain.reshape(1, columns), w_gate, w_up, w_down)
+            collective_id=0, has_side_effects=True, vmem_limit_bytes=66 * 1000 * 1000),
+        name="layer",
+    )(queries_small, queries_large, kv_small, kv_large, cum_small, cum_large, residual,
+      gain_mix.reshape(1, columns), gain_route.reshape(1, columns), route, bias.reshape(1, keep),
+      gain_blend.reshape(1, columns), out_small, out_large, w_gate, w_up, w_down)
 
 
 def on_device(
@@ -709,11 +683,10 @@
     route,
     route_bias,
 ):
-    mixed, routed = mix(
+    return layer(
         dims, queries_small, queries_large, kv_small, kv_large, cum_small, cum_large, residual,
-        gain_mix, gain_route, out_small, out_large,
+        gain_mix, gain_route, route, route_bias, gain_blend, out_small, out_large, w_gate, w_up, w_down,
     )
-    return experts_of(dims, routed, mixed, route, route_bias, gain_blend, w_gate, w_up, w_down)
 
 
 def solution(mesh):

time: 118 us -> 112 us (0.949)
  Pallas kernels: 116 us -> 110 us
    pallas_call x2 -> x1, Pallas kernels: 116 us -> 110 us  [layer(): pl.pallas_call(functools.partial(layer_kernel, dims, (heads_small, heads_...]
where the time goes in v3:
time: 112 us
  Pallas kernels  110 us (98%)
  local copies, waits for them, and re-layouts  1.88 us (2%)
    pallas_call x1, Pallas kernels, layer(): pl.pallas_call(functools.partial(layer_kernel, dims, (heads_small, heads_...  110 us

profile of v3, /device:TPU:0, one launch (start us, length us, event | category | flops | bytes accessed | tf_op | source)
XLA Modules:
  0.0 112.1 jit_solution(1301260962137560703)
XLA Ops:
  0.0 110.2 %layer.1 = bf16[128,2048]{1,0:T(8,128)(2,1)} custom-call(bf16[256,512]{1,0:T(8,128)(2,1)} %q_small.1, bf16[256,512]{1,0:T(8,128)(2,1)} %q_large.1, bf16[256,128]{1,0:T(8,128)(2,1)} %kv_small.1, bf16[256,256]{1,0:T(8,128)(2,1)} %kv_large.1, f32[8,256]{1,0:T(8,128)} %cum_small.1, f32[4,256]{1,0:T(4,128)} %cum_large.1, bf16[128,2048]{1,0:T(8,128)(2,1)} %residual.1, ...), custom_call_target="tpu_custom_call" | custom-call | tf_op jit(solution)/shard_map/layer/pallas_call | solution.py:627
  110.2 1.9 %copy.19 = bf16[128,2048]{1,0:T(8,128)(2,1)} copy(bf16[128,2048]{1,0:T(8,128)(2,1)} %layer.1) | data formatting | bytes 1048576

commit v4 on v3

--- a/solution.py
+++ b/solution.py
@@ -62,25 +62,31 @@
     return jnp.sum(jnp.where(eye, row, 0.0), axis=1, keepdims=True)
 
 
-def plan_of(depth):
-    if depth == 4:
+def plan_of(depth, parts):
+    if depth == 4 and parts == 2:
         texts = (
-            "E0 E1 F0 F1 E3 E2 F3 F2 C3 C2 C1 C0",
-            "E1 E0 E2 F1 F2 C2 C1 E3 F3 F0 C3 C0",
-            "E0 E2 E1 E3 F0 F2 F1 C0 F3 C1 C3 C2",
-            "E3 E1 E0 E2 F1 F3 C3 C1 F0 F2 C0 C2",
+            ("E00 E01 E10 E11 F0 F1 E20 E30 E21 E31 C10 F2 C11 F3 C20 C00 C01 C21 C30 C31", (3, 1, 2)),
+            ("E00 E01 E10 E20 E21 E11 F0 F2 C00 C20 E30 E31 C21 C01 F3 F1 C30 C10 C31 C11", (3, 2, 0)),
+            ("E20 E30 E10 E31 E11 E00 F3 C30 E01 F1 C31 E21 C10 F0 C11 F2 C00 C01 C20 C21", (1, 0, 3)),
+            ("E10 E11 E00 E01 F1 F0 E30 C00 C10 E20 C01 E21 E31 C11 F2 F3 C20 C21 C30 C31", (2, 0, 1)),
         )
-        return [[("EFC".index(word[0]), int(word[1])) for word in text.split()] for text in texts]
-    plans = []
+        kinds = {"F": 0, "E0": 1, "E1": 2, "C0": 3, "C1": 4}
+        plans = [[(kinds[word[0] + word[2:]], int(word[1])) for word in text.split()] for text, _ in texts]
+        return plans, [sends for _, sends in texts]
+    plans, sends = [], []
     for z in range(depth):
         order = [z + step for step in distances(depth) if 0 <= z + step < depth]
         plan = []
         for turn in range(depth + 2):
-            plan += [(0, order[turn])] if turn < depth else []
-            plan += [(1, order[turn - 1])] if 1 <= turn <= depth else []
-            plan += [(2, order[turn - 2])] if turn >= 2 else []
+            if turn < depth:
+                plan += [(1 + part, order[turn]) for part in range(parts)]
+            if 1 <= turn <= depth:
+                plan += [(0, order[turn - 1])]
+            if turn >= 2:
+                plan += [(1 + parts + part, order[turn - 2]) for part in range(parts)]
         plans.append(plan)
-    return plans
+        sends.append(order[1:])
+    return plans, sends
 
 
 def layer_kernel(
@@ -276,7 +282,7 @@
         return copies(me, (mine_z + step) * plane + me % plane, send_far.at[step])
 
     column(0)
-    for step in reversed(range(1, depth)):
+    for step in range(1, depth):
 
         def send_up(step=step):
             for copy in far(step):
@@ -330,7 +336,6 @@
                 acc_ref[number] = acc_ref[number] * factor[:, :size] + product
 
     attend(me, True)
-    pl.when(mine_z >= 1)(lambda: column(jnp.int32(1)))
     neighbours(0)
     order = [(0, 0)] + [(step, 0) for step in range(1, rows_y)] + [(0, step) for step in range(1, rows_x)]
     order += [(a, b) for a in range(1, rows_y) for b in range(1, rows_x)]
@@ -338,7 +343,7 @@
     def step_of(number, _):
         behind = number // plane
         turn = number % plane
-        pl.when((turn == 0) & (behind + 1 <= mine_z))(lambda: column(behind + 1))
+        pl.when((turn == jnp.where(behind == 0, min(1, plane - 1), 0)) & (behind + 1 <= mine_z))(lambda: column(behind + 1))
         pl.when(turn == min(2, plane - 1))(lambda: corners(behind))
         pl.when((turn == plane - 1) & (behind + 1 <= mine_z))(lambda: neighbours(behind + 1))
         off_y = jnp.int32(0)
@@ -390,13 +395,26 @@
         copy.start()
     for load in loads:
         load.wait()
+    span_w = 512
+
+    def half_product(which, span):
+        cols_s = pl.ds(pl.multiple_of(which * width_s, 128), width_s)
+        cols_l = pl.ds(pl.multiple_of(2 * width_s + which * width_l, 128), width_l)
+        return jnp.dot(whole[:, cols_s], weights[cols_s, span], preferred_element_type=jnp.float32) + jnp.dot(
+            whole[:, cols_l], weights[cols_l, span], preferred_element_type=jnp.float32)
+
+    def project_own(number, _):
+        span = pl.ds(pl.multiple_of(number * span_w, span_w), span_w)
+        mixer[:, span] = half_product(core, span)
+        return 0
+
+    lax.fori_loop(0, columns // span_w, project_own, 0)
     for copy in swap(1 - core):
         copy.wait_recv()
-    span_w = 512
 
     def project(number, squares):
         span = pl.ds(pl.multiple_of(number * span_w, span_w), span_w)
-        part = jnp.dot(whole[...], weights[:, span], preferred_element_type=jnp.float32)
+        part = mixer[:, span] + half_product(1 - core, span)
         mixer[:, span] = part
         square = part * part
         return squares + functools.reduce(jnp.add, [square[:, j * 128:(j + 1) * 128] for j in range(span_w // 128)])
@@ -418,75 +436,89 @@
     in_rows[mine_z] = out_rows[mine_z]
     metas[mine_z] = out_meta[mine_z]
 
-    def along(other, slot):
-        target = (other * plane + me % plane, core)
-        return (
-            pltpu.make_async_remote_copy(
-                src_ref=out_rows.at[other], dst_ref=in_rows.at[slot], send_sem=send_rows.at[other],
-                recv_sem=recv_rows.at[slot], device_id=target, device_id_type=MESH),
-            pltpu.make_async_remote_copy(
-                src_ref=out_meta.at[other], dst_ref=metas.at[slot], send_sem=send_meta.at[other],
-                recv_sem=recv_meta.at[slot], device_id=target, device_id_type=MESH),
-        )
-
-    def outward(source, other, slot):
+    parts = recv_rows.shape[1]
+    plans, sends = plan_of(depth, parts)
+    extent = columns // parts
+
+    def columns_of(part):
+        return pl.ds(part * extent, extent)
+
+    def along_rows(other, slot, part):
         return pltpu.make_async_remote_copy(
-            src_ref=spread.at[source, other], dst_ref=received.at[source, slot],
-            send_sem=send_block.at[source, other], recv_sem=recv_block.at[source, slot],
+            src_ref=out_rows.at[other, :, columns_of(part)], dst_ref=in_rows.at[slot, :, columns_of(part)],
+            send_sem=send_rows.at[other, part], recv_sem=recv_rows.at[slot, part],
+            device_id=(other * plane + me % plane, core), device_id_type=MESH)
+
+    def along_meta(other, slot):
+        return pltpu.make_async_remote_copy(
+            src_ref=out_meta.at[other], dst_ref=metas.at[slot], send_sem=send_meta.at[other],
+            recv_sem=recv_meta.at[slot], device_id=(other * plane + me % plane, core), device_id_type=MESH)
+
+    def outward(source, other, slot, part):
+        return pltpu.make_async_remote_copy(
+            src_ref=spread.at[source, other, :, columns_of(part)],
+            dst_ref=received.at[source, slot, :, columns_of(part)],
+            send_sem=send_block.at[source, other, part], recv_sem=recv_block.at[source, slot, part],
             device_id=(mine_z * plane + other // cores, other % cores), device_id_type=MESH)
 
-    def inward(source, other, slot):
+    def inward(source, other, slot, part):
         return pltpu.make_async_remote_copy(
-            src_ref=outs.at[source, other], dst_ref=back.at[source, slot],
-            send_sem=send_back.at[source, other], recv_sem=recv_back.at[source, slot],
+            src_ref=outs.at[source, other, :, columns_of(part)],
+            dst_ref=back.at[source, slot, :, columns_of(part)],
+            send_sem=send_back.at[source, other, part], recv_sem=recv_back.at[source, slot, part],
             device_id=(mine_z * plane + other // cores, other % cores), device_id_type=MESH)
 
-    def homeward(other, slot):
+    def homeward(other, slot, part):
         return pltpu.make_async_remote_copy(
-            src_ref=combined.at[other], dst_ref=final.at[slot], send_sem=send_home.at[other],
-            recv_sem=recv_home.at[slot], device_id=(other * plane + me % plane, core), device_id_type=MESH)
+            src_ref=combined.at[other, :, columns_of(part)], dst_ref=final.at[slot, :, columns_of(part)],
+            send_sem=send_home.at[other, part], recv_sem=recv_home.at[slot, part],
+            device_id=(other * plane + me % plane, core), device_id_type=MESH)
 
     steps = distances(depth)
-    for step in steps[1:]:
-        other = mine_z + step
-
-        def launch(other=other):
-            for copy in along(other, mine_z):
-                copy.start()
-
-        pl.when((other >= 0) & (other < depth))(launch)
-
-    def flat(ref, source):
+    for index in range(depth - 1):
+        other = jnp.int32(0)
+        for z in range(depth):
+            other = jnp.where(mine_z == z, sends[z][index], other)
+        along_meta(other, mine_z).start()
+        for part in range(parts):
+            along_rows(other, mine_z, part).start()
+
+    def flat(ref, source, span):
         if capacity % 16:
             return jnp.concatenate(
-                [ref[source, lane].astype(jnp.float32) for lane in range(lanes)], axis=0).astype(jnp.bfloat16)
-        return ref[source].reshape(count, columns)
+                [ref[source, lane, :, span].astype(jnp.float32) for lane in range(lanes)], axis=0).astype(jnp.bfloat16)
+        found = ref[source, :, :, span]
+        return found.reshape(count, found.shape[2])
 
     def split(ref, source, values, span):
         for lane in range(lanes):
             ref[source, lane, :, span] = values[lane * capacity:(lane + 1) * capacity].astype(jnp.bfloat16)
 
-    def expand(source):
+    def expand(source, part):
+        span = columns_of(part)
+
         def landed():
-            for copy in along(source, source):
-                copy.wait_recv()
+            if part == 0:
+                along_meta(source, source).wait_recv()
+            along_rows(source, source, part).wait_recv()
 
         pl.when(source != mine_z)(landed)
         wanted = lax.broadcasted_iota(jnp.int32, (count, slots), 0).astype(jnp.float32) + 1.0
         spots = jnp.where(
             (wanted == metas[source, 0:1, :slots]) | (wanted == metas[source, 1:2, :slots]), 1.0, 0.0
         ).astype(jnp.bfloat16)
-        split(spread, source, jnp.dot(spots, in_rows[source], preferred_element_type=jnp.float32), slice(None))
-        received[source, here] = spread[source, here]
+        split(spread, source, jnp.dot(spots, in_rows[source, :, span], preferred_element_type=jnp.float32), span)
+        received[source, here, :, span] = spread[source, here, :, span]
         for move in range(1, lanes):
-            outward(source, (here + move) % lanes, here).start()
+            outward(source, (here + move) % lanes, here, part).start()
 
     tile = 256
 
     def compute(source):
-        for move in range(1, lanes):
-            outward(source, (here + move) % lanes, (here + move) % lanes).wait_recv()
-        rows = flat(received, source)
+        for part in range(parts):
+            for move in range(1, lanes):
+                outward(source, (here + move) % lanes, (here + move) % lanes, part).wait_recv()
+        rows = flat(received, source, slice(None))
 
         def enter(number, _):
             span = pl.ds(pl.multiple_of(number * tile, tile), tile)
@@ -496,41 +528,43 @@
             return 0
 
         lax.fori_loop(0, gate_w.shape[1] // tile, enter, 0)
-
-        def leave(number, _):
-            span = pl.ds(pl.multiple_of(number * 2 * tile, 2 * tile), 2 * tile)
-            split(outs, source, jnp.dot(hidden[...], down_w[:, span], preferred_element_type=jnp.float32), span)
-            return 0
-
-        lax.fori_loop(0, columns // (2 * tile), leave, 0)
-        back[source, here] = outs[source, here]
+        for part in range(parts):
+
+            def leave(number, _):
+                span = pl.ds(pl.multiple_of(part * extent + number * 2 * tile, 2 * tile), 2 * tile)
+                split(outs, source, jnp.dot(hidden[...], down_w[:, span], preferred_element_type=jnp.float32), span)
+                return 0
+
+            lax.fori_loop(0, extent // (2 * tile), leave, 0)
+            span = columns_of(part)
+            back[source, here, :, span] = outs[source, here, :, span]
+            for move in range(1, lanes):
+                inward(source, (here + move) % lanes, here, part).start()
+
+    def combine(source, part):
+        span = columns_of(part)
         for move in range(1, lanes):
-            inward(source, (here + move) % lanes, here).start()
-
-    def combine(source):
-        for move in range(1, lanes):
-            inward(source, (here + move) % lanes, (here + move) % lanes).wait_recv()
+            inward(source, (here + move) % lanes, (here + move) % lanes, part).wait_recv()
         wanted = lax.broadcasted_iota(jnp.int32, (count, width), 0).astype(jnp.float32) + 1.0
         shares = jnp.where(wanted == metas[source, 0:1, :], metas[source, 2:3, :], 0.0)
         shares = shares + jnp.where(wanted == metas[source, 1:2, :], metas[source, 3:4, :], 0.0)
         shares = shares.T[:slots]
         high = shares.astype(jnp.bfloat16)
         low = (shares - high.astype(jnp.float32)).astype(jnp.bfloat16)
-        picked = flat(back, source)
+        picked = flat(back, source, span)
         mixed = jnp.dot(high, picked, preferred_element_type=jnp.float32) + jnp.dot(
             low, picked, preferred_element_type=jnp.float32)
 
         def away():
-            combined[source] = mixed.astype(jnp.bfloat16)
-            homeward(source, mine_z).start()
+            combined[source, :, span] = mixed.astype(jnp.bfloat16)
+            homeward(source, mine_z, part).start()
 
         def stay():
-            final[source] = mixed.astype(jnp.bfloat16)
+            final[source, :, span] = mixed.astype(jnp.bfloat16)
 
         pl.when(source != mine_z)(away)
         pl.when(source == mine_z)(stay)
 
-    plans = plan_of(depth)
 
     def turn_of(turn, _):
         found = jnp.int32(0)
@@ -539,28 +573,31 @@
                 found = jnp.where((mine_z == z) & (turn == index), kind * depth + source, found)
         kind = found // depth
         source = found % depth
-        pl.when(kind == 0)(lambda: expand(source))
-        pl.when(kind == 1)(lambda: compute(source))
-        pl.when(kind == 2)(lambda: combine(source))
+        pl.when(kind == 0)(lambda: compute(source))
+        for part in range(parts):
+            pl.when(kind == 1 + part)(functools.partial(expand, source, part))
+            pl.when(kind == 1 + parts + part)(functools.partial(combine, source, part))
         return 0
 
     for load in expert_loads:
         load.wait()
-    lax.fori_loop(0, 3 * depth, turn_of, 0)
+    lax.fori_loop(0, (1 + 2 * parts) * depth, turn_of, 0)
     for step in steps[1:]:
         other = mine_z + step
 
         def settle(other=other):
-            homeward(other, other).wait_recv()
-            homeward(other, mine_z).wait_send()
-            for copy in along(other, mine_z):
-                copy.wait_send()
+            along_meta(other, mine_z).wait_send()
+            for part in range(parts):
+                homeward(other, other, part).wait_recv()
+                homeward(other, mine_z, part).wait_send()
+                along_rows(other, mine_z, part).wait_send()
 
         pl.when((other >= 0) & (other < depth))(settle)
     for source in range(depth):
         for move in range(1, lanes):
-            outward(source, (here + move) % lanes, here).wait_send()
-            inward(source, (here + move) % lanes, here).wait_send()
+            for part in range(parts):
+                outward(source, (here + move) % lanes, here, part).wait_send()
+                inward(source, (here + move) % lanes, here, part).wait_send()
     for step in range(1, depth):
 
         def sent_up(step=step):
@@ -595,6 +632,12 @@
     result_ref[...] = (
         mixed_ref[...].astype(jnp.float32) + rms_scale(blended, gain_ref[...])
     ).astype(jnp.bfloat16)
+
+
+def padded_bytes(item):
+    size = jnp.dtype(item.dtype).itemsize if jnp.issubdtype(item.dtype, jnp.floating) else 0
+    lead = math.prod(item.shape[:-2]) if len(item.shape) > 1 else 0
+    return size * lead * round_up(item.shape[-2], 32 // max(size, 1)) * round_up(item.shape[-1], 128) if lead else 0
 
 
 def layer(dims, queries_small, queries_large, kv_small, kv_large, cum_small, cum_large, residual, gain_mix, gain_route, route, bias, gain_blend, out_small, out_large, w_gate, w_up, w_down):
@@ -615,6 +658,7 @@
     capacity = 4 * keep // (depth * lanes)
     slots = capacity * lanes // 2
     width = round_up(slots, 128)
+    parts = 2
     inner = w_gate.shape[2]
     joined = out_small.shape[0] + out_large.shape[0]
     dma = pltpu.SemaphoreType.DMA
@@ -624,39 +668,41 @@
     rows = pltpu.VMEM((depth, slots, columns), bf16)
     blocks = pltpu.VMEM((depth, lanes, capacity, columns), bf16)
     meta = pltpu.VMEM((depth, 8, width), f32)
+    scratch = [
+        pltpu.VMEM((shards, table_rows, tokens), bf16),
+        pltpu.VMEM((shards, heads, tokens), f32),
+        pltpu.VMEM((heads_small, tokens, extra_s + size_small), bf16),
+        pltpu.VMEM((heads_large, tokens, size_large + extra_l), bf16),
+        pltpu.VMEM((heads, tokens, 128), f32),
+        pltpu.VMEM((heads, tokens, 128), f32),
+        pltpu.VMEM((heads_small, tokens, size_small), f32),
+        pltpu.VMEM((heads_large, tokens, size_large), f32),
+        pltpu.VMEM((keep, heads_small * size_small + heads_large * size_large), bf16),
+        pltpu.VMEM((keep, joined), bf16),
+        pltpu.VMEM((joined, columns), bf16),
+        pltpu.VMEM((keep, columns), f32),
+        pltpu.VMEM((keep, columns), bf16),
+        pltpu.VMEM((8, keep), f32),
+        rows, rows, meta, meta, blocks, blocks, blocks, blocks, rows, rows,
+        pltpu.VMEM((lanes * capacity, inner), bf16),
+        pltpu.VMEM((columns, inner), bf16),
+        pltpu.VMEM((columns, inner), bf16),
+        pltpu.VMEM((inner, columns), bf16),
+        dma((depth, 2)), dma((depth, near, 2)), dma((shards,)), dma((shards,)), dma((shards,)), dma((shards,)),
+        dma((2,)), dma((2,)), dma((5,)),
+        dma((depth, parts)), dma((depth, parts)), dma((depth,)), dma((depth,)),
+        dma((depth, lanes, parts)), dma((depth, lanes, parts)), dma((depth, lanes, parts)), dma((depth, lanes, parts)),
+        dma((depth, parts)), dma((depth, parts)),
+    ]
+    needed = sum(padded_bytes(item) for item in scratch if isinstance(item, type(rows)))
     return pl.pallas_call(
         functools.partial(layer_kernel, dims, (heads_small, heads_large, size_small, size_large)),
         out_shape=jax.ShapeDtypeStruct(residual.shape, bf16),
         in_specs=[vmem] * 12 + [hbm] * 5,
         out_specs=vmem,
-        scratch_shapes=[
-            pltpu.VMEM((shards, table_rows, tokens), bf16),
-            pltpu.VMEM((shards, heads, tokens), f32),
-            pltpu.VMEM((heads_small, tokens, extra_s + size_small), bf16),
-            pltpu.VMEM((heads_large, tokens, size_large + extra_l), bf16),
-            pltpu.VMEM((heads, tokens, 128), f32),
-            pltpu.VMEM((heads, tokens, 128), f32),
-            pltpu.VMEM((heads_small, tokens, size_small), f32),
-            pltpu.VMEM((heads_large, tokens, size_large), f32),
-            pltpu.VMEM((keep, heads_small * size_small + heads_large * size_large), bf16),
-            pltpu.VMEM((keep, joined), bf16),
-            pltpu.VMEM((joined, columns), bf16),
-            pltpu.VMEM((keep, columns), f32),
-            pltpu.VMEM((keep, columns), bf16),
-            pltpu.VMEM((8, keep), f32),
-            rows, rows, meta, meta, blocks, blocks, blocks, blocks, rows, rows,
-            pltpu.VMEM((lanes * capacity, inner), bf16),
-            pltpu.VMEM((columns, inner), bf16),
-            pltpu.VMEM((columns, inner), bf16),
-            pltpu.VMEM((inner, columns), bf16),
-            dma((depth, 2)), dma((depth, near, 2)), dma((shards,)), dma((shards,)), dma((shards,)), dma((shards,)),
-            dma((2,)), dma((2,)), dma((5,)),
-            dma((depth,)), dma((depth,)), dma((depth,)), dma((depth,)),
-            dma((depth, lanes)), dma((depth, lanes)), dma((depth, lanes)), dma((depth, lanes)),
-            dma((depth,)), dma((depth,)),
-        ],
+        scratch_shapes=scratch,
         compiler_params=pltpu.CompilerParams(
-            collective_id=0, has_side_effects=True, vmem_limit_bytes=66 * 1000 * 1000),
+            collective_id=0, has_side_effects=True, vmem_limit_bytes=min(needed + 4 * 1024 * 1024, 66 * 1000 * 1000)),
         name="layer",
     )(queries_small, queries_large, kv_small, kv_large, cum_small, cum_large, residual,
       gain_mix.reshape(1, columns), gain_route.reshape(1, columns), route, bias.reshape(1, keep),

time: 112 us -> 112 us (level)
  the two profiles are of different devices: /device:TPU:0 before, /device:TPU:9 now
where the time goes in v4:
time: 112 us; the launch traced here: 111 us
  Pallas kernels  98 us (88%)
  local copies, waits for them, and re-layouts  12.5 us (11%)
    pallas_call x1, Pallas kernels, layer(): pl.pallas_call(functools.partial(layer_kernel, dims, (heads_small, heads_...  98 us
    unnamed x27, local copies, waits for them, and re-layouts  12.5 us

profile of v4, /device:TPU:9, one launch (start us, length us, event | category | flops | bytes accessed | tf_op | source)
XLA Modules:
  0.0 110.5 jit_solution(16678404360067047716)
XLA Ops:
  0.0 0.0 copy-start
  0.0 2.2 %copy-done = bf16[1024,2048]{1,0:T(8,128)(2,1)S(1)} copy-done((bf16[1024,2048]{1,0:T(8,128)(2,1)S(1)}, bf16[1024,2048]{1,0:T(8,128)(2,1)}, u32[]{:S(2)}) %copy-start) | copy-done | bytes 4194328
  2.2 0.0 copy-start.1
  2.2 1.0 copy-done.1
  3.2 0.0 copy-start.2
  3.2 0.9 copy-done.2
  4.2 0.0 copy-start.3
  4.2 0.9 copy-done.3
  5.1 0.0 copy-start.4
  5.1 0.9 copy-done.4
  6.0 0.0 copy-start.5
  6.0 0.8 copy-done.5
  6.9 0.0 copy-start.6
  6.9 0.7 copy-done.6
  7.6 0.0 copy-start.7
  7.6 0.7 copy-done.7
  8.3 0.0 copy-start.8
  8.3 0.7 copy-done.8
  9.0 0.0 copy-start.9
  9.0 0.7 copy-done.9
  9.7 0.0 copy-start.10
  9.7 0.7 copy-done.10
  10.4 0.0 copy-start.11
  10.4 0.7 copy-done.11
  11.0 0.0 copy-start.12
  11.0 0.7 copy-done.12
  11.7 98.0 %layer.1 = bf16[128,2048]{1,0:T(8,128)(2,1)S(1)} custom-call(bf16[256,512]{1,0:T(8,128)(2,1)S(1)} %copy-done.2, bf16[256,512]{1,0:T(8,128)(2,1)S(1)} %copy-done.3, bf16[256,128]{1,0:T(8,128)(2,1)S(1)} %copy-done.5, bf16[256,256]{1,0:T(8,128)(2,1)S(1)} %copy-done.4, f32[8,256]{1,0:T(8,128)S(1)} %copy-done.6, f32[4,256]{1,0:T(4,128)S(1)} %copy-done.10, ...), custom_call_target="tpu_custom_call" | custom-call | tf_op jit(solution)/shard_map/layer/pallas_call | solution.py:698
  109.7 0.8 copy.19
Async XLA Ops:
  0.0 2.2 %copy-start = (bf16[1024,2048]{1,0:T(8,128)(2,1)S(1)}, bf16[1024,2048]{1,0:T(8,128)(2,1)}, u32[]{:S(2)}) copy-start(bf16[1024,2048]{1,0:T(8,128)(2,1)} %out_small.1) | copy-start | bytes 12582916
  2.2 1.0 copy-start.1
  3.2 0.9 copy-start.2
  4.2 0.9 copy-start.3
  5.1 0.9 copy-start.4
  6.0 0.8 copy-start.5
  6.9 0.7 copy-start.6
  7.6 0.7 copy-start.7
  8.3 0.7 copy-start.8
  9.0 0.7 copy-start.9
  9.7 0.7 copy-start.10
  10.4 0.7 copy-start.11
  11.0 0.7 copy-start.12

commit v5 on v4

--- a/solution.py
+++ b/solution.py
@@ -91,13 +91,14 @@
 
 def layer_kernel(
     dims, head_shape,
-    q_small, q_large, kv_small, kv_large, cum_small, cum_large, residual, gain_mix, gain_route, route_ref, bias_ref, gain_ref,
+    q_small_in, q_large_in, kv_small_in, kv_large_in, cum_small_in, cum_large_in, residual_in, gain_mix_in, gain_route_in, route_ref_in, bias_ref_in, gain_ref_in,
     out_small, out_large, w_gate, w_up, w_down,
     result_ref,
+    q_small, q_large, kv_small, kv_large, cum_small, cum_large, residual, gain_mix, gain_route, route_ref, bias_ref, gain_ref,
     table, cums, qs, ql, top, total, acc_s, acc_l, stage, whole, weights, mixer, mixed_ref, routing,
     out_rows, in_rows, out_meta, metas, spread, received, outs, back, combined, final, hidden, gate_w, up_w, down_w,
     send_far, send_near, send_core, recv_kv, recv_cum, recv_core, swap_send, swap_recv, load_sem,
-    send_rows, recv_rows, send_meta, recv_meta, send_block, recv_block, send_back, recv_back, send_home, recv_home,
+    operand_sem, send_rows, recv_rows, send_meta, recv_meta, send_block, recv_block, send_back, recv_back, send_home, recv_home,
 ):
     heads_small, heads_large, size_small, size_large = head_shape
     depth, rows_y, rows_x = dims
@@ -135,9 +136,17 @@
         pltpu.make_async_copy(w_up.at[0], up_w, load_sem.at[3]),
         pltpu.make_async_copy(w_down.at[0], down_w, load_sem.at[4]),
     )
-    for load in loads + expert_loads:
-        load.start()
+    moved = (
+        (kv_small_in, kv_small), (kv_large_in, kv_large), (cum_small_in, cum_small), (cum_large_in, cum_large),
+        (route_ref_in, route_ref), (bias_ref_in, bias_ref), (q_small_in, q_small), (q_large_in, q_large),
+        (residual_in, residual), (gain_mix_in, gain_mix), (gain_route_in, gain_route), (gain_ref_in, gain_ref),
+    )
+    moves = [pltpu.make_async_copy(source, target, operand_sem.at[n]) for n, (source, target) in enumerate(moved)]
+    for move in moves:
+        move.start()
     greeted = greet(depth, plane, cores, me, core)
+    for move in moves[:4]:
+        move.wait()
     def turned(block):
         width = block.shape[1]
         eye = jnp.where(
@@ -152,6 +161,10 @@
     cums[me, :heads_small] = cum_small[...]
     cums[me, heads_small:heads] = cum_large[...]
 
+    for move in moves[4:]:
+        move.wait()
+    for load in loads + expert_loads:
+        load.start()
     lanes_s = lax.broadcasted_iota(jnp.int32, (tokens, extra_s), 1)
     lanes_l = lax.broadcasted_iota(jnp.int32, (tokens, extra_l), 1)
     for h in range(heads_small):
@@ -634,12 +647,6 @@
     ).astype(jnp.bfloat16)
 
 
-def padded_bytes(item):
-    size = jnp.dtype(item.dtype).itemsize if jnp.issubdtype(item.dtype, jnp.floating) else 0
-    lead = math.prod(item.shape[:-2]) if len(item.shape) > 1 else 0
-    return size * lead * round_up(item.shape[-2], 32 // max(size, 1)) * round_up(item.shape[-1], 128) if lead else 0
-
-
 def layer(dims, queries_small, queries_large, kv_small, kv_large, cum_small, cum_large, residual, gain_mix, gain_route, route, bias, gain_blend, out_small, out_large, w_gate, w_up, w_down):
     shards = lax.axis_size("sp")
     depth, rows_y, rows_x = dims
@@ -663,12 +670,24 @@
     joined = out_small.shape[0] + out_large.shape[0]
     dma = pltpu.SemaphoreType.DMA
     vmem = pl.BlockSpec(memory_space=pltpu.VMEM)
-    hbm = pl.BlockSpec(memory_space=pl.ANY)
+    hbm = pl.BlockSpec(memory_space=pltpu.HBM)
     bf16, f32 = jnp.bfloat16, jnp.float32
     rows = pltpu.VMEM((depth, slots, columns), bf16)
     blocks = pltpu.VMEM((depth, lanes, capacity, columns), bf16)
     meta = pltpu.VMEM((depth, 8, width), f32)
     scratch = [
+        pltpu.VMEM(queries_small.shape, bf16),
+        pltpu.VMEM(queries_large.shape, bf16),
+        pltpu.VMEM(kv_small.shape, bf16),
+        pltpu.VMEM(kv_large.shape, bf16),
+        pltpu.VMEM(cum_small.shape, f32),
+        pltpu.VMEM(cum_large.shape, f32),
+        pltpu.VMEM(residual.shape, bf16),
+        pltpu.VMEM((1, columns), f32),
+        pltpu.VMEM((1, columns), f32),
+        pltpu.VMEM(route.shape, route.dtype),
+        pltpu.VMEM((1, keep), f32),
+        pltpu.VMEM((1, columns), f32),
         pltpu.VMEM((shards, table_rows, tokens), bf16),
         pltpu.VMEM((shards, heads, tokens), f32),
         pltpu.VMEM((heads_small, tokens, extra_s + size_small), bf16),
@@ -689,20 +708,19 @@
         pltpu.VMEM((columns, inner), bf16),
         pltpu.VMEM((inner, columns), bf16),
         dma((depth, 2)), dma((depth, near, 2)), dma((shards,)), dma((shards,)), dma((shards,)), dma((shards,)),
-        dma((2,)), dma((2,)), dma((5,)),
+        dma((2,)), dma((2,)), dma((5,)), dma((12,)),
         dma((depth, parts)), dma((depth, parts)), dma((depth,)), dma((depth,)),
         dma((depth, lanes, parts)), dma((depth, lanes, parts)), dma((depth, lanes, parts)), dma((depth, lanes, parts)),
         dma((depth, parts)), dma((depth, parts)),
     ]
-    needed = sum(padded_bytes(item) for item in scratch if isinstance(item, type(rows)))
     return pl.pallas_call(
         functools.partial(layer_kernel, dims, (heads_small, heads_large, size_small, size_large)),
         out_shape=jax.ShapeDtypeStruct(residual.shape, bf16),
-        in_specs=[vmem] * 12 + [hbm] * 5,
+        in_specs=[hbm] * 17,
         out_specs=vmem,
         scratch_shapes=scratch,
         compiler_params=pltpu.CompilerParams(
-            collective_id=0, has_side_effects=True, vmem_limit_bytes=min(needed + 4 * 1024 * 1024, 66 * 1000 * 1000)),
+            collective_id=0, has_side_effects=True, vmem_limit_bytes=66 * 1000 * 1000),
         name="layer",
     )(queries_small, queries_large, kv_small, kv_large, cum_small, cum_large, residual,
       gain_mix.reshape(1, columns), gain_route.reshape(1, columns), route, bias.reshape(1, keep),

time: 112 us -> 101 us (0.902)
  local copies, waits for them, and re-layouts: 12.5 us -> 1.88 us
    unnamed x27 -> x1, local copies, waits for them, and re-layouts: 12.5 us -> 1.88 us
where the time goes in v5:
time: 101 us
  Pallas kernels  98.7 us (98%)
  local copies, waits for them, and re-layouts  1.88 us (2%)
    pallas_call x1, Pallas kernels, layer(): pl.pallas_call(functools.partial(layer_kernel, dims, (heads_small, heads_...  98.7 us

profile of v5, /device:TPU:9, one launch (start us, length us, event | category | flops | bytes accessed | tf_op | source)
XLA Modules:
  0.0 100.6 jit_solution(9752482041668459150)
XLA Ops:
  0.0 98.7 %layer.1 = bf16[128,2048]{1,0:T(8,128)(2,1)} custom-call(bf16[256,512]{1,0:T(8,128)(2,1)} %q_small_in.1, bf16[256,512]{1,0:T(8,128)(2,1)} %q_large_in.1, bf16[256,128]{1,0:T(8,128)(2,1)} %kv_small_in.1, bf16[256,256]{1,0:T(8,128)(2,1)} %kv_large_in.1, f32[8,256]{1,0:T(8,128)} %cum_small_in.1, f32[4,256]{1,0:T(4,128)} %cum_large_in.1, ...), custom_call_target="tpu_custom_call" | custom-call | tf_op jit(solution)/shard_map/layer/pallas_call | solution.py:716
  98.7 1.9 %copy.19 = bf16[128,2048]{1,0:T(8,128)(2,1)} copy(bf16[128,2048]{1,0:T(8,128)(2,1)} %layer.1) | data formatting | bytes 1048576

commit v6 on v5

--- a/solution.py
+++ b/solution.py
@@ -64,15 +64,14 @@
 
 def plan_of(depth, parts):
     if depth == 4 and parts == 2:
-        texts = (
-            ("E00 E01 E10 E11 F0 F1 E20 E30 E21 E31 C10 F2 C11 F3 C20 C00 C01 C21 C30 C31", (3, 1, 2)),
-            ("E00 E01 E10 E20 E21 E11 F0 F2 C00 C20 E30 E31 C21 C01 F3 F1 C30 C10 C31 C11", (3, 2, 0)),
-            ("E20 E30 E10 E31 E11 E00 F3 C30 E01 F1 C31 E21 C10 F0 C11 F2 C00 C01 C20 C21", (1, 0, 3)),
-            ("E10 E11 E00 E01 F1 F0 E30 C00 C10 E20 C01 E21 E31 C11 F2 F3 C20 C21 C30 C31", (2, 0, 1)),
+        coded = (
+            (5, 4, 9, 6, 10, 1, 2, 14, 13, 7, 11, 18, 8, 17, 3, 0, 15, 19, 12, 16),
+            (5, 4, 8, 0, 9, 7, 11, 6, 10, 3, 1, 15, 12, 19, 2, 13, 16, 14, 17, 18),
+            (6, 5, 9, 4, 8, 10, 0, 1, 12, 13, 16, 7, 11, 3, 17, 2, 15, 19, 14, 18),
+            (4, 8, 6, 5, 9, 7, 10, 1, 2, 11, 13, 14, 17, 0, 18, 3, 12, 16, 15, 19),
         )
-        kinds = {"F": 0, "E0": 1, "E1": 2, "C0": 3, "C1": 4}
-        plans = [[(kinds[word[0] + word[2:]], int(word[1])) for word in text.split()] for text, _ in texts]
-        return plans, [sends for _, sends in texts]
+        sends = ((3, 1, 2), (2, 0, 3), (0, 3, 1), (2, 1, 0))
+        return [[(code // depth, code % depth) for code in plan] for plan in coded], sends
     plans, sends = [], []
     for z in range(depth):
         order = [z + step for step in distances(depth) if 0 <= z + step < depth]

time: 101 us -> 97.4 us (0.964)
  the two profiles are of different devices: /device:TPU:9 before, /device:TPU:0 now
where the time goes in v6:
time: 97.4 us; the launch traced here: 97.2 us
  Pallas kernels  95.4 us (98%)
  local copies, waits for them, and re-layouts  1.88 us (2%)
    pallas_call x1, Pallas kernels, layer(): pl.pallas_call(functools.partial(layer_kernel, dims, (heads_small, heads_...  95.4 us

profile of v6, /device:TPU:0, one launch (start us, length us, event | category | flops | bytes accessed | tf_op | source)
XLA Modules:
  0.0 97.2 jit_solution(901391067499039114)
XLA Ops:
  0.0 95.4 %layer.1 = bf16[128,2048]{1,0:T(8,128)(2,1)} custom-call(bf16[256,512]{1,0:T(8,128)(2,1)} %q_small_in.1, bf16[256,512]{1,0:T(8,128)(2,1)} %q_large_in.1, bf16[256,128]{1,0:T(8,128)(2,1)} %kv_small_in.1, bf16[256,256]{1,0:T(8,128)(2,1)} %kv_large_in.1, f32[8,256]{1,0:T(8,128)} %cum_small_in.1, f32[4,256]{1,0:T(4,128)} %cum_large_in.1, ...), custom_call_target="tpu_custom_call" | custom-call | tf_op jit(solution)/shard_map/layer/pallas_call | solution.py:715
  95.4 1.9 %copy.19 = bf16[128,2048]{1,0:T(8,128)(2,1)} copy(bf16[128,2048]{1,0:T(8,128)(2,1)} %layer.1) | data formatting | bytes 1048576
